TPU v7x, 32 devices: a whole 2x2x4 slice. The times are simulated.
32 devices in a mesh: sp: 8 (over z, y), dp: 4 (over x, core).
Axes of the slice: x: 2, y: 2, z: 4, core: 2. Of those that a mesh axis runs over, the one named last changes fastest.
Arguments:
- queries: bfloat16 [4, 2048, 1280], P('dp', None, 'sp'), may hold values from -6 to 6
- keys: bfloat16 [4, 1024, 1280], P('dp', None, 'sp'), may hold values from -6 to 6
- values: bfloat16 [4, 1024, 1280], P('dp', None, 'sp'), may hold values from -48 to 48
- q_gain: float32 [64], replicated, may hold values from 0.5 to 10
- k_gain: float32 [64], replicated, may hold values from 0.5 to 10
- w_out: bfloat16 [2048, 2048], P(None, 'dp'), may hold values from -0.125 to 0.125
Outputs:
- mixed: bfloat16 [4, 1280, 2048], P('dp', 'sp')
All inputs are finite; a program needn't handle non-finite values.
Results may differ from a plain program's by a relative error of at most 0.0038.
The roundings to bfloat16 on the way count: a program that leaves them out, or rounds other values in their place, can miss the bound.
Values may be sent and summed in bfloat16 or wider, within the bound.
A program may use at most 64 MiB of HBM per device.

v0:
```python
import functools

import jax
import jax.numpy as jnp
from jax import lax
from jax.experimental import pallas as pl
from jax.experimental.pallas import tpu as pltpu
from jax.sharding import PartitionSpec as P

HD = 64
QH = 32
KV = 16
GRID_W = 64


epsilon = 1e-06
rotary_base = 10000.0
block_count = 8


def swapped(block, axis, apart):
    count = lax.axis_size(axis)
    route = []
    for low in range(count):
        high = low | 1 << apart
        if high != low and high < count:
            route += [(low, high), (high, low)]
    return lax.ppermute(block, axis, route)


def rotary_tables(first_row, row_count):
    position = first_row + lax.iota(jnp.int32, row_count)
    grid_row = (position // GRID_W).astype(jnp.float32)
    grid_col = (position % GRID_W).astype(jnp.float32)
    quarter = HD // 4
    inv_freq = rotary_base ** (-(2.0 * lax.iota(jnp.float32, quarter)) / (HD // 2))
    row_angle = inv_freq[:, None] * grid_row[None, :]
    col_angle = inv_freq[:, None] * grid_col[None, :]
    cos_table = jnp.concatenate(
        [jnp.cos(row_angle), jnp.cos(row_angle), jnp.cos(col_angle), jnp.cos(col_angle)], axis=0
    )
    sin_table = jnp.concatenate(
        [jnp.sin(row_angle), jnp.sin(row_angle), jnp.sin(col_angle), jnp.sin(col_angle)], axis=0
    )
    return (cos_table, sin_table)


def normalize_turn(field, gain, cos_table, sin_table):
    head_count = field.shape[0] // HD
    values_f = field.astype(jnp.float32).reshape(head_count, HD, field.shape[1])
    normed = (
        values_f
        * lax.rsqrt(jnp.mean(values_f * values_f, axis=1, keepdims=True) + epsilon)
        * gain[None, :, None]
    )
    quarter = HD // 4
    quarters_of = normed.reshape(head_count, 4, quarter, field.shape[1])
    turned = jnp.concatenate(
        [-quarters_of[:, 1], quarters_of[:, 0], -quarters_of[:, 3], quarters_of[:, 2]], axis=1
    )
    return (normed * cos_table[None] + turned * sin_table[None]).astype(jnp.bfloat16)


def attention_heads(query_heads, key_heads, value_heads, seq_len):
    kv_local = key_heads.shape[0]
    group_local = query_heads.shape[0] // kv_local
    query_split = query_heads.reshape(kv_local, group_local, HD, seq_len)
    score_scale = HD ** (-0.5)
    block_rows = seq_len // block_count

    def one_block(block_index, result):
        row_start = block_index * block_rows
        query_block = lax.dynamic_slice_in_dim(query_split, row_start, block_rows, 3)
        scores = (
            jnp.einsum("hgdq,hdk->hgqk", query_block, key_heads, preferred_element_type=jnp.float32)
            * score_scale
        )
        row_max = jnp.max(scores, axis=-1, keepdims=True)
        weights = jnp.exp(scores - row_max)
        weights = (weights / jnp.sum(weights, axis=-1, keepdims=True)).astype(jnp.bfloat16)
        attended = jnp.einsum(
            "hgqk,hdk->hgdq", weights, value_heads, preferred_element_type=jnp.float32
        )
        return lax.dynamic_update_slice_in_dim(result, attended.astype(jnp.bfloat16), row_start, 3)

    result = jnp.zeros(query_split.shape, jnp.bfloat16)
    result = lax.fori_loop(0, block_count, one_block, result)
    return result.reshape(query_heads.shape)


def on_device_plain(queries, keys, values, q_gain, k_gain, w_out):
    sp_count = lax.axis_size("sp")
    tok_rows = queries.shape[2]
    seq_len = tok_rows * sp_count
    cos_table, sin_table = rotary_tables(lax.axis_index("sp") * tok_rows, tok_rows)
    query_rot = normalize_turn(queries[0], q_gain, cos_table, sin_table)
    key_rot = normalize_turn(keys[0], k_gain, cos_table, sin_table)
    value_rows = values[0].reshape(KV, HD, tok_rows)
    query_heads = lax.all_to_all(query_rot, "sp", split_axis=0, concat_axis=2, tiled=True)
    share_count = max(sp_count // KV, 1)
    part_rows = tok_rows // share_count
    key_cut = (
        key_rot.reshape(KV, HD, share_count, part_rows)
        .transpose(0, 2, 1, 3)
        .reshape(KV * share_count, HD, part_rows)
    )
    value_cut = (
        value_rows.reshape(KV, HD, share_count, part_rows)
        .transpose(0, 2, 1, 3)
        .reshape(KV * share_count, HD, part_rows)
    )
    key_got, value_got = (
        lax.all_to_all(key_cut, "sp", split_axis=0, concat_axis=2, tiled=True),
        lax.all_to_all(value_cut, "sp", split_axis=0, concat_axis=2, tiled=True),
    )
    kv_local = key_got.shape[0]
    key_got = key_got.reshape(kv_local, HD, sp_count, part_rows)
    value_got = value_got.reshape(kv_local, HD, sp_count, part_rows)
    for bit_index in range(share_count.bit_length() - 1):
        key_other, value_other = swapped((key_got, value_got), "sp", bit_index)
        key_got = jnp.concatenate([key_got, key_other], axis=3)
        value_got = jnp.concatenate([value_got, value_other], axis=3)
    key_heads = key_got.reshape(kv_local, HD, seq_len)
    value_heads = value_got.reshape(kv_local, HD, seq_len)
    attended = attention_heads(query_heads, key_heads, value_heads, seq_len)
    token_heads = lax.all_to_all(attended, "sp", split_axis=2, concat_axis=0, tiled=True)
    token_rows = token_heads.reshape(QH * HD, tok_rows)
    product = lax.dot_general(
        token_rows,
        lax.all_gather(w_out, "dp", axis=1, tiled=True),
        (((0,), (0,)), ((), ())),
        preferred_element_type=jnp.float32,
    )
    mixed_rows = product.astype(jnp.bfloat16)
    return mixed_rows[None]


MESH = pl.DeviceIdType.MESH
LOG2E = 1.4426950408889634


def layer_kernel(
    n, m, q_ref, k_ref, v_ref, qg_ref, kg_ref, cos_ref, sin_ref, w_ref, out_ref,
    q_out, k_out, q_in, k_in, v_in, a_out, a_in, w_all,
    q_send, q_recv, k_send, k_recv, v_send, v_recv, a_send, a_recv, w_send, w_recv, w_pass, w_own,
):
    me = lax.axis_index("sp")
    dp = lax.axis_index("dp")
    x_count = m // 2
    core = lax.rem(dp, 2)
    x_at = dp // 2
    partner = x_at * 2 + (1 - core)
    rows = q_ref.shape[0]
    w_rows = w_ref.shape[0] // n
    kv_width = k_out.shape[2]
    pairs = kv_width // 128
    group = q_out.shape[2] // kv_width

    def at_sp(d):
        return lax.rem(me + d, n)

    def at_dp(d):
        return lax.rem(x_at + d, x_count) * 2 + core

    barrier = pltpu.get_barrier_semaphore()

    def greet(d, carry):
        pl.semaphore_signal(barrier, inc=1, device_id={"sp": at_sp(d)}, device_id_type=MESH)
        return carry

    lax.fori_loop(1, n, greet, 0)
    for d in range(1, x_count):
        pl.semaphore_signal(barrier, inc=1, device_id={"dp": at_dp(d)}, device_id_type=MESH)
    pl.semaphore_signal(barrier, inc=1, device_id={"dp": partner}, device_id_type=MESH)
    pl.semaphore_wait(barrier, n - 1 + x_count)

    def w_piece(shard, c):
        return w_all.at[shard, pl.ds(pl.multiple_of(c * w_rows, w_rows), w_rows)]

    def w_source(c):
        return w_ref.at[pl.ds(pl.multiple_of(c * w_rows, w_rows), w_rows)]

    def w_copy(d, c):
        return pltpu.make_async_remote_copy(
            src_ref=w_source(c), dst_ref=w_piece(dp, c), send_sem=w_send.at[d, c],
            recv_sem=w_recv.at[dp, c], device_id={"dp": at_dp(d) if d else partner},
            device_id_type=MESH,
        )

    def w_came(shard, c):
        return pltpu.make_async_remote_copy(
            src_ref=w_source(c), dst_ref=w_piece(shard, c), send_sem=w_send.at[0, c],
            recv_sem=w_recv.at[shard, c], device_id={"dp": partner}, device_id_type=MESH,
        )

    def w_forward(d, c):
        shard = at_dp(d)
        return pltpu.make_async_remote_copy(
            src_ref=w_piece(shard, c), dst_ref=w_piece(shard, c), send_sem=w_pass.at[d, c],
            recv_sem=w_recv.at[shard, c], device_id={"dp": partner}, device_id_type=MESH,
        )

    def start_w(c, carry):
        for d in range(x_count):
            w_copy(d, c).start()
        return carry

    lax.fori_loop(0, n, start_w, 0)
    own_w = pltpu.make_async_copy(w_ref, w_all.at[dp], w_own)
    own_w.start()

    lane = lax.broadcasted_iota(jnp.int32, (rows, 128), 1)
    low = lane < HD
    even = (lane // (HD // 4)) % 2 == 0
    q_gain, k_gain = (jnp.concatenate([g[...], g[...]], axis=1) for g in (qg_ref, kg_ref))

    def turn(tile, gain):
        u = tile.astype(jnp.float32)
        square = u * u
        sum_low = jnp.sum(jnp.where(low, square, 0.0), axis=1, keepdims=True)
        sum_high = jnp.sum(jnp.where(low, 0.0, square), axis=1, keepdims=True)
        inverse = jnp.where(
            low, lax.rsqrt(sum_low * (1.0 / HD) + epsilon), lax.rsqrt(sum_high * (1.0 / HD) + epsilon)
        )
        normed = u * inverse * gain
        part = HD // 4
        turned = jnp.where(even, pltpu.roll(normed, 128 - part, 1), pltpu.roll(normed, part, 1))
        return normed * cos_ref[...] + turned * sin_ref[...]

    def crossed(first, second):
        one = jnp.where(low, first, pltpu.roll(second, HD, 1))
        two = jnp.where(low, pltpu.roll(first, HD, 1), second)
        return one, two

    def exchange(out, into, send, recv, d):
        peer = at_sp(d)
        return pltpu.make_async_remote_copy(
            src_ref=out.at[peer], dst_ref=into.at[me], send_sem=send.at[peer],
            recv_sem=recv.at[me], device_id={"sp": peer}, device_id_type=MESH,
        )

    def arrival(out, into, send, recv, source):
        return pltpu.make_async_remote_copy(
            src_ref=out.at[source], dst_ref=into.at[source], send_sem=send.at[source],
            recv_sem=recv.at[source], device_id={"sp": source}, device_id_type=MESH,
        )

    def kv_lanes(peer, j=0, size=kv_width):
        return pl.ds(pl.multiple_of(peer * kv_width + j * 128, 128), size)

    def turn_keys(peer, into, at):
        for j in range(pairs):
            tile = turn(k_ref[:, kv_lanes(peer, j, 128)], k_gain)
            into[at, :, j * 128 : (j + 1) * 128] = tile.astype(jnp.bfloat16)

    def turn_queries(peer, into, at):
        base = peer * (kv_width * group)
        for j in range(pairs):
            natural = [
                turn(q_ref[:, pl.ds(pl.multiple_of(base + j * 256 + i * 128, 128), 128)], q_gain)
                for i in range(2)
            ]
            for g, tile in enumerate(crossed(*natural)):
                start = g * kv_width + j * 128
                into[at, :, start : start + 128] = tile.astype(jnp.bfloat16)

    def send_values(d):
        peer = at_sp(d)
        return pltpu.make_async_remote_copy(
            src_ref=v_ref.at[:, kv_lanes(peer)], dst_ref=v_in.at[me], send_sem=v_send.at[peer],
            recv_sem=v_recv.at[me], device_id={"sp": peer}, device_id_type=MESH,
        )

    def send_kv(d, carry):
        peer = at_sp(d)
        send_values(d).start()
        turn_keys(peer, k_out, peer)
        exchange(k_out, k_in, k_send, k_recv, d).start()
        return carry

    def send_q(d, carry):
        peer = at_sp(d)
        turn_queries(peer, q_out, peer)
        exchange(q_out, q_in, q_send, q_recv, d).start()
        return carry

    lax.fori_loop(1, n, send_kv, 0)
    lax.fori_loop(1, n, send_q, 0)
    turn_keys(me, k_in, me)
    v_in[me] = v_ref[:, kv_lanes(me)]
    turn_queries(me, q_in, me)

    def await_kv(d, carry):
        source = at_sp(d)
        arrival(k_out, k_in, k_send, k_recv, source).wait_recv()
        arrival(k_out, v_in, v_send, v_recv, source).wait_recv()
        return carry

    lax.fori_loop(1, n, await_kv, 0)
    seq_len = n * rows
    scale = HD ** (-0.5) * LOG2E

    def attend(source):
        for j in range(pairs):
            keys = k_in[:, :, j * 128 : (j + 1) * 128].reshape(seq_len, 128)
            vals = v_in[:, :, j * 128 : (j + 1) * 128].reshape(seq_len, 128)
            tiles = []
            for g in range(group):
                at = g * kv_width + j * 128
                pair = q_in[source, :, at : at + 128]
                zero = jnp.zeros_like(pair)
                both = []
                for one in (jnp.where(low, pair, zero), jnp.where(low, zero, pair)):
                    s = lax.dot_general(
                        one, keys, (((1,), (1,)), ((), ())), preferred_element_type=jnp.float32
                    )
                    p = jnp.exp2((s - jnp.max(s, axis=1, keepdims=True)) * scale)
                    p = p * (1.0 / jnp.sum(p, axis=1, keepdims=True))
                    both.append(
                        jnp.dot(p.astype(jnp.bfloat16), vals, preferred_element_type=jnp.float32)
                    )
                tiles.append(jnp.where(low, both[0], both[1]))
            yield j, jnp.concatenate(crossed(*tiles), axis=1).astype(jnp.bfloat16)

    def block(d, carry):
        source = at_sp(d)
        arrival(q_out, q_in, q_send, q_recv, source).wait_recv()
        for j, tile in attend(source):
            a_out[source, :, j * 256 : (j + 1) * 256] = tile
        exchange(a_out, a_in, a_send, a_recv, d).start()
        for e in range(1, x_count):
            w_came(at_dp(e), d - 1).wait_recv()
            w_forward(e, d - 1).start()
        return carry

    lax.fori_loop(1, n, block, 0)
    for j, tile in attend(me):
        a_in[me, :, j * 256 : (j + 1) * 256] = tile
    own_w.wait()

    def came(d, carry):
        source = at_sp(d)
        arrival(a_out, a_in, a_send, a_recv, source).wait_recv()
        return carry

    lax.fori_loop(1, n, came, 0)
    width = w_ref.shape[1]

    def product(shard):
        total = jnp.zeros((rows, width), jnp.float32)
        step = a_in.shape[2]
        for p in range(n):
            total += jnp.dot(
                a_in[p], w_all[shard, p * step : (p + 1) * step, :],
                preferred_element_type=jnp.float32,
            )
        out_ref[:, pl.ds(pl.multiple_of(shard * width, width), width)] = total.astype(jnp.bfloat16)

    def await_w(shard):
        def one(c, carry):
            w_came(shard, c).wait_recv()
            return carry

        lax.fori_loop(0, n, one, 0)

    product(dp)
    await_w(partner)
    product(partner)
    for e in range(1, x_count):
        w_came(at_dp(e), n - 1).wait_recv()
        w_forward(e, n - 1).start()
    for e in range(1, x_count):
        product(at_dp(e))
    for e in range(1, x_count):
        other = at_dp(e) + 1 - 2 * core
        await_w(other)
        product(other)

    def sent(d, carry):
        exchange(k_out, k_in, k_send, k_recv, d).wait_send()
        send_values(d).wait_send()
        exchange(q_out, q_in, q_send, q_recv, d).wait_send()
        exchange(a_out, a_in, a_send, a_recv, d).wait_send()
        return carry

    lax.fori_loop(1, n, sent, 0)

    def sent_w(c, carry):
        for d in range(x_count):
            w_copy(d, c).wait_send()
        for d in range(1, x_count):
            w_forward(d, c).wait_send()
        return carry

    lax.fori_loop(0, n, sent_w, 0)


def rotary_lanes(first_row, row_count):
    position = first_row + lax.broadcasted_iota(jnp.int32, (row_count, 128), 0)
    lane = lax.broadcasted_iota(jnp.int32, (row_count, 128), 1)
    place = jnp.where(lane % HD < HD // 2, position // GRID_W, position % GRID_W)
    quarter = HD // 4
    step = (lax.iota(jnp.int32, 128) % quarter).astype(jnp.float32)
    inv_freq = rotary_base ** (-(2.0 * step) / (HD // 2))
    angle = inv_freq[None, :] * place.astype(jnp.float32)
    sign = jnp.where((lane // quarter) % 2 == 0, -1.0, 1.0)
    return (jnp.cos(angle), jnp.sin(angle) * sign)


def on_device(queries, keys, values, q_gain, k_gain, w_out):
    n, m = lax.axis_size("sp"), lax.axis_size("dp")
    tok_rows = queries.shape[2]
    kv_width = keys.shape[1] // n
    if kv_width % 128 or m % 2 or tok_rows % 16 or QH != 2 * KV:
        return on_device_plain(queries, keys, values, q_gain, k_gain, w_out)
    q_width = queries.shape[1] // n
    cos_table, sin_table = rotary_lanes(lax.axis_index("sp") * tok_rows, tok_rows)
    vmem = pl.BlockSpec(memory_space=pltpu.VMEM)
    bf16 = jnp.bfloat16
    dma = pltpu.SemaphoreType.DMA
    mixed = pl.pallas_call(
        functools.partial(layer_kernel, n, m),
        out_shape=jax.ShapeDtypeStruct((tok_rows, w_out.shape[1] * m), bf16),
        in_specs=[vmem] * 7 + [pl.BlockSpec(memory_space=pltpu.HBM)],
        out_specs=vmem,
        scratch_shapes=[
            pltpu.VMEM((n, tok_rows, q_width), bf16),
            pltpu.VMEM((n, tok_rows, kv_width), bf16),
            pltpu.VMEM((n, tok_rows, q_width), bf16),
            pltpu.VMEM((n, tok_rows, kv_width), bf16),
            pltpu.VMEM((n, tok_rows, kv_width), bf16),
            pltpu.VMEM((n, tok_rows, q_width), bf16),
            pltpu.VMEM((n, tok_rows, q_width), bf16),
            pltpu.VMEM((m, w_out.shape[0], w_out.shape[1]), bf16),
        ]
        + [dma((n,))] * 8
        + [dma((m // 2, n)), dma((m, n)), dma((m // 2, n)), dma],
        compiler_params=pltpu.CompilerParams(
            collective_id=0, has_side_effects=True, vmem_limit_bytes=48 * 1024 * 1024
        ),
    )(
        queries[0].T, keys[0].T, values[0].T, q_gain[None], k_gain[None],
        cos_table, sin_table, w_out,
    )
    return mixed[None]


def solution(mesh):
    placed = (
        P("dp", None, "sp"),
        P("dp", None, "sp"),
        P("dp", None, "sp"),
        P(),
        P(),
        P(None, "dp"),
    )
    return jax.shard_map(
        on_device, mesh=mesh, in_specs=placed, out_specs=P("dp", "sp", None), check_vma=False
    )
```

profile of v0, /device:TPU:9, one launch (start us, length us, event | category | flops | bytes accessed | tf_op | source)
XLA Modules:
  0.0 70.8 jit_solution(11019069260312852620)
XLA Ops:
  0.1 0.4 select_multiply_fusion
  0.5 0.0 copy-start
  0.5 1.6 %copy-done = bf16[2048,512]{1,0:T(8,128)(2,1)S(1)} copy-done((bf16[2048,512]{1,0:T(8,128)(2,1)S(1)}, bf16[2048,512]{1,0:T(8,128)(2,1)}, u32[]{:S(2)}) %copy-start) | copy-done | bytes 2097176
  2.1 0.0 copy-start.1
  2.1 1.1 %copy-done.1 = bf16[1,2048,160]{1,2,0:T(8,128)(2,1)S(1)} copy-done((bf16[1,2048,160]{1,2,0:T(8,128)(2,1)S(1)}, bf16[1,2048,160]{1,2,0:T(8,128)(2,1)}, u32[]{:S(2)}) %copy-start.1) | copy-done | bytes 655384
  3.2 0.0 copy-start.2
  3.2 1.0 %copy-done.2 = bf16[1,1024,160]{1,2,0:T(8,128)(2,1)S(1)} copy-done((bf16[1,1024,160]{1,2,0:T(8,128)(2,1)S(1)}, bf16[1,1024,160]{1,2,0:T(8,128)(2,1)}, u32[]{:S(2)}) %copy-start.2) | copy-done | bytes 327704
  4.2 0.0 copy-start.3
  4.2 1.0 %copy-done.3 = bf16[1,1024,160]{1,2,0:T(8,128)(2,1)S(1)} copy-done((bf16[1,1024,160]{1,2,0:T(8,128)(2,1)S(1)}, bf16[1,1024,160]{1,2,0:T(8,128)(2,1)}, u32[]{:S(2)}) %copy-start.3) | copy-done | bytes 327704
  5.1 0.0 copy-start.4
  5.1 0.7 copy-done.4
  5.8 0.0 copy-start.5
  5.8 0.7 copy-done.5
  6.5 63.5 %shard_map.64 = bf16[160,2048]{1,0:T(8,128)(2,1)S(1)} custom-call(bf16[160,2048]{1,0:T(8,128)(2,1)S(1)} %bitcast.13, bf16[160,1024]{1,0:T(8,128)(2,1)S(1)} %bitcast.14, bf16[160,1024]{1,0:T(8,128)(2,1)S(1)} %bitcast.15, f32[1,64]{1,0:T(1,128)S(1)} %bitcast.16, f32[1,64]{1,0:T(1,128)S(1)} %bitcast.17, f32[160,128]{1,0:T(8,128)S(1)} %get-tuple-element.6.cos_ref, ...), custom_call_target="tpu_custom_call" | custom-call | tf_op jit(solution)/shard_map/pallas_call | solution.py:421
  69.9 0.8 %copy.8 = bf16[1,160,2048]{2,1,0:T(8,128)(2,1)} copy(bf16[1,160,2048]{2,1,0:T(8,128)(2,1)S(1)} %bitcast.12) | data formatting | bytes 1310720
  (7 shorter events, 0.1 us)
Async XLA Ops:
  0.5 1.6 %copy-start = (bf16[2048,512]{1,0:T(8,128)(2,1)S(1)}, bf16[2048,512]{1,0:T(8,128)(2,1)}, u32[]{:S(2)}) copy-start(bf16[2048,512]{1,0:T(8,128)(2,1)} %w_ref.1) | copy-start | bytes 6291460
  2.1 1.1 %copy-start.1 = (bf16[1,2048,160]{1,2,0:T(8,128)(2,1)S(1)}, bf16[1,2048,160]{1,2,0:T(8,128)(2,1)}, u32[]{:S(2)}) copy-start(bf16[1,2048,160]{1,2,0:T(8,128)(2,1)} %param.6) | copy-start | bytes 1966084
  3.2 1.0 %copy-start.2 = (bf16[1,1024,160]{1,2,0:T(8,128)(2,1)S(1)}, bf16[1,1024,160]{1,2,0:T(8,128)(2,1)}, u32[]{:S(2)}) copy-start(bf16[1,1024,160]{1,2,0:T(8,128)(2,1)} %param.7) | copy-start | bytes 983044
  4.2 1.0 %copy-start.3 = (bf16[1,1024,160]{1,2,0:T(8,128)(2,1)S(1)}, bf16[1,1024,160]{1,2,0:T(8,128)(2,1)}, u32[]{:S(2)}) copy-start(bf16[1,1024,160]{1,2,0:T(8,128)(2,1)} %param.8) | copy-start | bytes 983044
  5.1 0.7 copy-start.4
  5.8 0.7 copy-start.5
where the time goes:
time: 71.1 us; the launch traced here: 70.8 us
  Pallas kernels  63.5 us (89%)
  local copies, waits for them, and re-layouts  6.77 us (10%)
    pallas_call x1, Pallas kernels, on_device(): pl.pallas_call(functools.partial(layer_kernel, n, m), out_shape=jax.Shape...  63.5 us
    unnamed x13, local copies, waits for them, and re-layouts  6.77 us

commit v1 on v0

v1 whole, which is shorter than its diff:
```python
import functools

import jax
import jax.numpy as jnp
import numpy as np
from jax import lax
from jax.experimental import pallas as pl
from jax.experimental.pallas import tpu as pltpu
from jax.sharding import PartitionSpec as P

HD = 64
QH = 32
KV = 16
GRID_W = 64


epsilon = 1e-06
rotary_base = 10000.0
block_count = 8


def swapped(block, axis, apart):
    count = lax.axis_size(axis)
    route = []
    for low in range(count):
        high = low | 1 << apart
        if high != low and high < count:
            route += [(low, high), (high, low)]
    return lax.ppermute(block, axis, route)


def rotary_tables(first_row, row_count):
    position = first_row + lax.iota(jnp.int32, row_count)
    grid_row = (position // GRID_W).astype(jnp.float32)
    grid_col = (position % GRID_W).astype(jnp.float32)
    quarter = HD // 4
    inv_freq = rotary_base ** (-(2.0 * lax.iota(jnp.float32, quarter)) / (HD // 2))
    row_angle = inv_freq[:, None] * grid_row[None, :]
    col_angle = inv_freq[:, None] * grid_col[None, :]
    cos_table = jnp.concatenate(
        [jnp.cos(row_angle), jnp.cos(row_angle), jnp.cos(col_angle), jnp.cos(col_angle)], axis=0
    )
    sin_table = jnp.concatenate(
        [jnp.sin(row_angle), jnp.sin(row_angle), jnp.sin(col_angle), jnp.sin(col_angle)], axis=0
    )
    return (cos_table, sin_table)


def normalize_turn(field, gain, cos_table, sin_table):
    head_count = field.shape[0] // HD
    values_f = field.astype(jnp.float32).reshape(head_count, HD, field.shape[1])
    normed = (
        values_f
        * lax.rsqrt(jnp.mean(values_f * values_f, axis=1, keepdims=True) + epsilon)
        * gain[None, :, None]
    )
    quarter = HD // 4
    quarters_of = normed.reshape(head_count, 4, quarter, field.shape[1])
    turned = jnp.concatenate(
        [-quarters_of[:, 1], quarters_of[:, 0], -quarters_of[:, 3], quarters_of[:, 2]], axis=1
    )
    return (normed * cos_table[None] + turned * sin_table[None]).astype(jnp.bfloat16)


def attention_heads(query_heads, key_heads, value_heads, seq_len):
    kv_local = key_heads.shape[0]
    group_local = query_heads.shape[0] // kv_local
    query_split = query_heads.reshape(kv_local, group_local, HD, seq_len)
    score_scale = HD ** (-0.5)
    block_rows = seq_len // block_count

    def one_block(block_index, result):
        row_start = block_index * block_rows
        query_block = lax.dynamic_slice_in_dim(query_split, row_start, block_rows, 3)
        scores = (
            jnp.einsum("hgdq,hdk->hgqk", query_block, key_heads, preferred_element_type=jnp.float32)
            * score_scale
        )
        row_max = jnp.max(scores, axis=-1, keepdims=True)
        weights = jnp.exp(scores - row_max)
        weights = (weights / jnp.sum(weights, axis=-1, keepdims=True)).astype(jnp.bfloat16)
        attended = jnp.einsum(
            "hgqk,hdk->hgdq", weights, value_heads, preferred_element_type=jnp.float32
        )
        return lax.dynamic_update_slice_in_dim(result, attended.astype(jnp.bfloat16), row_start, 3)

    result = jnp.zeros(query_split.shape, jnp.bfloat16)
    result = lax.fori_loop(0, block_count, one_block, result)
    return result.reshape(query_heads.shape)


def on_device_plain(queries, keys, values, q_gain, k_gain, w_out):
    sp_count = lax.axis_size("sp")
    tok_rows = queries.shape[2]
    seq_len = tok_rows * sp_count
    cos_table, sin_table = rotary_tables(lax.axis_index("sp") * tok_rows, tok_rows)
    query_rot = normalize_turn(queries[0], q_gain, cos_table, sin_table)
    key_rot = normalize_turn(keys[0], k_gain, cos_table, sin_table)
    value_rows = values[0].reshape(KV, HD, tok_rows)
    query_heads = lax.all_to_all(query_rot, "sp", split_axis=0, concat_axis=2, tiled=True)
    share_count = max(sp_count // KV, 1)
    part_rows = tok_rows // share_count
    key_cut = (
        key_rot.reshape(KV, HD, share_count, part_rows)
        .transpose(0, 2, 1, 3)
        .reshape(KV * share_count, HD, part_rows)
    )
    value_cut = (
        value_rows.reshape(KV, HD, share_count, part_rows)
        .transpose(0, 2, 1, 3)
        .reshape(KV * share_count, HD, part_rows)
    )
    key_got, value_got = (
        lax.all_to_all(key_cut, "sp", split_axis=0, concat_axis=2, tiled=True),
        lax.all_to_all(value_cut, "sp", split_axis=0, concat_axis=2, tiled=True),
    )
    kv_local = key_got.shape[0]
    key_got = key_got.reshape(kv_local, HD, sp_count, part_rows)
    value_got = value_got.reshape(kv_local, HD, sp_count, part_rows)
    for bit_index in range(share_count.bit_length() - 1):
        key_other, value_other = swapped((key_got, value_got), "sp", bit_index)
        key_got = jnp.concatenate([key_got, key_other], axis=3)
        value_got = jnp.concatenate([value_got, value_other], axis=3)
    key_heads = key_got.reshape(kv_local, HD, seq_len)
    value_heads = value_got.reshape(kv_local, HD, seq_len)
    attended = attention_heads(query_heads, key_heads, value_heads, seq_len)
    token_heads = lax.all_to_all(attended, "sp", split_axis=2, concat_axis=0, tiled=True)
    token_rows = token_heads.reshape(QH * HD, tok_rows)
    product = lax.dot_general(
        token_rows,
        lax.all_gather(w_out, "dp", axis=1, tiled=True),
        (((0,), (0,)), ((), ())),
        preferred_element_type=jnp.float32,
    )
    mixed_rows = product.astype(jnp.bfloat16)
    return mixed_rows[None]


MESH = pl.DeviceIdType.MESH
LOG2E = 1.4426950408889634
LANES = 128
TRANSPOSED = (((1,), (1,)), ((), ()))


def layer_kernel(
    m, q_ref, k_ref, v_ref, qg_ref, kg_ref, cos_ref, sin_ref, w_ref, out_ref,
    q_raw, k_raw, q_gain_in, k_gain_in, cos_in, sin_in, k_out, q_out, kv_in, q_in, a_out, a_in,
    w_all, score, peak, inv_sum,
    load, v_own, k_side, v_side, q_side, k_got, v_got, q_got, kv_up, q_up, kv_mid, kv_got,
    a_send, a_got, w_x, w_y, w_core, w_got, w_local,
):
    me = lax.axis_index("sp")
    dp = lax.axis_index("dp")
    z, y = me // 2, me % 2
    half = z // 2
    z_in, z_out = 1 + half, 3 * half
    inner = z == z_in
    outer = jnp.logical_not(inner)
    base = jnp.where(inner, 0, 2)
    mine, beside = base + y, base + 1 - y
    sibling = z * 2 + 1 - y
    in_same = z_in * 2 + y
    across = (3 - z_in) * 2 + y
    core = lax.rem(dp, 2)
    x_at = dp // 2
    x_peer = (1 - x_at) * 2 + core
    core_peer = x_at * 2 + 1 - core
    x_other = (1 - x_at) * 2 + 1 - core
    rows = k_raw.shape[0]
    pairs = kv_in.shape[0]
    parts = 2 * pairs
    w_rows = w_ref.shape[0] // parts

    barrier = pltpu.get_barrier_semaphore()

    def greet(**there):
        pl.semaphore_signal(barrier, inc=1, device_id=there, device_id_type=MESH)

    greet(sp=sibling)
    greet(dp=x_peer)
    greet(dp=core_peer)
    z_other = jnp.where(inner, z_out, z_in)
    greet(sp=z_other * 2 + y)
    greet(sp=z_other * 2 + 1 - y)

    @pl.when(inner)
    def _():
        greet(sp=across)

    def kv_lanes(side, j):
        return pl.ds(pl.multiple_of((side * pairs + j) * LANES, LANES), LANES)

    first = pl.multiple_of(me * rows, rows)
    loads = [
        pltpu.make_async_copy(k_ref, k_raw, load.at[0]),
        pltpu.make_async_copy(cos_ref.at[pl.ds(first, rows)], cos_in, load.at[1]),
        pltpu.make_async_copy(sin_ref.at[pl.ds(first, rows)], sin_in, load.at[2]),
        pltpu.make_async_copy(kg_ref, k_gain_in, load.at[3]),
        pltpu.make_async_copy(qg_ref, q_gain_in, load.at[4]),
        pltpu.make_async_copy(q_ref, q_raw, load.at[5]),
    ]
    for one in loads:
        one.start()

    def own_values(j):
        return pltpu.make_async_copy(
            v_ref.at[:, kv_lanes(y, j)], kv_in.at[j, mine, 1], v_own.at[j]
        )

    for j in range(pairs):
        own_values(j).start()
    own_w = pltpu.make_async_copy(w_ref, w_all.at[dp], w_local)
    own_w.start()

    def remote(src, dst, sent, got, **there):
        return pltpu.make_async_remote_copy(
            src_ref=src, dst_ref=dst, send_sem=sent, recv_sem=got,
            device_id=there, device_id_type=MESH,
        )

    def k_aside(j, to=None):
        to = mine if to is None else to
        return remote(k_out.at[j], kv_in.at[j, to, 0], k_side.at[j], k_got.at[j], sp=sibling)

    def v_aside(j, to=None):
        to = mine if to is None else to
        return remote(
            v_ref.at[:, kv_lanes(1 - y, j)], kv_in.at[j, to, 1], v_side.at[j], v_got.at[j],
            sp=sibling,
        )

    def q_aside(j, to=None):
        to = mine if to is None else to
        return remote(q_out.at[j], q_in.at[j, to], q_side.at[j], q_got.at[j, to], sp=sibling)

    def kv_upward(j, s):
        return remote(
            kv_in.at[j, s], kv_in.at[j, s], kv_up.at[j, s], kv_got.at[j, s], sp=in_same
        )

    def q_upward(j, s):
        return remote(q_in.at[j, s], q_in.at[j, s], q_up.at[j, s], q_got.at[j, s], sp=in_same)

    def kv_across(j, s):
        return remote(
            kv_in.at[j, s], kv_in.at[j, 4 + s], kv_mid.at[j, s], kv_got.at[j, 4 + s], sp=across
        )

    def kv_came(j, s):
        remote(
            kv_in.at[j, s], kv_in.at[j, s], kv_up.at[j, 0], kv_got.at[j, s], sp=across
        ).wait_recv()

    def q_came(j, s):
        remote(q_in.at[j, s], q_in.at[j, s], q_up.at[j, 0], q_got.at[j, s], sp=sibling).wait_recv()

    def w_piece(ref, c):
        return ref.at[pl.ds(pl.multiple_of(c * w_rows, w_rows), w_rows)]

    def w_held(shard, c):
        return w_all.at[shard, pl.ds(pl.multiple_of(c * w_rows, w_rows), w_rows)]

    direct = parts - 2

    def part_at(i):
        if i < 2:
            return y * pairs + i
        return (i % 2) * pairs + 1 + i // 2

    def w_cross(i):
        c = part_at(i)
        return remote(w_piece(w_ref, c), w_held(dp, c), w_x.at[i], w_got.at[dp, c], dp=x_peer)

    def w_own_core():
        return remote(w_ref, w_all.at[dp], w_core.at[parts], w_got.at[dp, parts], dp=core_peer)

    def w_to_core(c):
        return remote(
            w_held(x_peer, c), w_held(x_peer, c), w_core.at[c], w_got.at[x_peer, c], dp=core_peer
        )

    def w_aside(i):
        c = part_at(i)
        return remote(
            w_held(x_peer, c), w_held(x_peer, c), w_y.at[i], w_got.at[x_peer, c], sp=sibling
        )

    def w_came(shard, c):
        remote(
            w_held(shard, c), w_held(shard, c), w_y.at[0], w_got.at[shard, c], dp=core_peer
        ).wait_recv()

    def pass_w(i):
        c = part_at(i)
        w_came(x_peer, c)
        w_to_core(c).start()
        if i < 2:
            w_aside(i).start()

    def pass_w_aside(i):
        c = (1 - y) * pairs + i
        w_came(x_peer, c)
        w_to_core(c).start()

    lane = lax.broadcasted_iota(jnp.int32, (rows, LANES), 1)
    low = lane < HD
    even = (lane // (HD // 4)) % 2 == 0

    def turn(tile, gain):
        u = tile.astype(jnp.float32)
        square = u * u
        sum_low = jnp.sum(jnp.where(low, square, 0.0), axis=1, keepdims=True)
        sum_high = jnp.sum(jnp.where(low, 0.0, square), axis=1, keepdims=True)
        inverse = jnp.where(
            low, lax.rsqrt(sum_low * (1.0 / HD) + epsilon), lax.rsqrt(sum_high * (1.0 / HD) + epsilon)
        )
        normed = u * inverse * gain
        part = HD // 4
        turned = jnp.where(even, pltpu.roll(normed, LANES - part, 1), pltpu.roll(normed, part, 1))
        return normed * cos_in[...] + turned * sin_in[...]

    def crossed(one, two):
        return (
            jnp.where(low, one, pltpu.roll(two, HD, 1)),
            jnp.where(low, pltpu.roll(one, HD, 1), two),
        )

    def turn_keys(j, side):
        return turn(k_raw[:, kv_lanes(side, j)], k_gain).astype(jnp.bfloat16)

    def turn_queries(j, side):
        at = (side * pairs + j) * 2 * LANES
        natural = [
            turn(q_raw[:, pl.ds(pl.multiple_of(at + i * LANES, LANES), LANES)], q_gain)
            for i in range(2)
        ]
        return jnp.concatenate(crossed(*natural), axis=1).astype(jnp.bfloat16)

    for one in loads[:5]:
        one.wait()
    q_gain, k_gain = (
        jnp.concatenate([g[...], g[...]], axis=1) for g in (q_gain_in, k_gain_in)
    )

    def key_step(j):
        k_out[j] = turn_keys(j, 1 - y)
        kv_in[j, mine, 0] = turn_keys(j, y)

    def query_step(j):
        q_out[j] = turn_queries(j, 1 - y)
        q_in[j, mine] = turn_queries(j, y)

    key_step(0)
    pl.semaphore_wait(barrier, jnp.where(inner, 6, 5))
    loads[5].wait()

    def send_step(j, carry):
        v_aside(j).start()

        @pl.when(j > 0)
        def _():
            key_step(j)

        k_aside(j).start()
        own_values(j).wait()

        @pl.when(jnp.logical_and(outer, j == 0))
        def _():
            kv_upward(j, mine).start()

        @pl.when(jnp.logical_and(inner, j < 2))
        def _():
            kv_across(j, mine).start()

        query_step(j)
        q_aside(j).start()

        @pl.when(jnp.logical_and(outer, j == 0))
        def _():
            q_upward(j, mine).start()

        return carry

    w_cross(0).start()
    w_cross(1).start()
    lax.fori_loop(0, pairs, send_step, 0)
    for i in range(2, direct):
        w_cross(i).start()
    w_own_core().start()

    def beside_came(j):
        k_aside(j, beside).wait_recv()
        v_aside(j, beside).wait_recv()

    @pl.when(outer)
    def _():
        def kv(j):
            if j:
                kv_upward(j, mine).start()
            beside_came(j)
            kv_upward(j, beside).start()

        def query(j):
            if j:
                q_upward(j, mine).start()
            q_came(j, beside)
            q_upward(j, beside).start()

        kv(0)
        query(0)
        for j in range(1, pairs):
            kv(j)
            if j > 1:
                query(j - 1)
        query(pairs - 1)
        for i in range(direct):
            pass_w(i)
            if i in (2, 3):
                pass_w_aside(i - 2)

    scale = HD ** (-0.5) * LOG2E
    step = 2 * LANES
    seq_len = 8 * rows
    tiles = [(t, min(step, seq_len - t)) for t in range(0, seq_len, step)]

    def halves(tile, op):
        parts_of = [tile[:, i : i + LANES] for i in range(0, tile.shape[1], LANES)]
        return functools.reduce(op, parts_of)

    def wide(column, size):
        return jnp.concatenate([column] * (size // LANES), axis=1)

    def multiply_scores(j, s, at):
        stack = []
        for g in range(2):
            pair = q_in[j, s, :, g * LANES : (g + 1) * LANES]
            zero = jnp.zeros_like(pair)
            stack += [jnp.where(low, pair, zero), jnp.where(low, zero, pair)]
        stack = jnp.concatenate(stack, axis=0)
        keys = kv_in[j, :, 0].reshape(seq_len, LANES)
        top = None
        for t, size in tiles:
            tile = lax.dot_general(
                stack, keys[t : t + size], TRANSPOSED, preferred_element_type=jnp.float32
            )
            score[at, :, t : t + size] = tile
            most = halves(tile, jnp.maximum)
            top = most if top is None else jnp.maximum(top, most)
        peak[at] = jnp.broadcast_to(jnp.max(top, axis=1, keepdims=True), top.shape)

    def exponents(at):
        top = peak[at]
        total = None
        for t, size in tiles:
            p = jnp.exp2((score[at, :, t : t + size] - wide(top, size)) * scale)
            score[at, :, t : t + size] = p
            more = halves(p, jnp.add)
            total = more if total is None else total + more
        inv_sum[at] = jnp.broadcast_to(1.0 / jnp.sum(total, axis=1, keepdims=True), total.shape)

    def weigh(j, at):
        inv = inv_sum[at]
        p = jnp.concatenate(
            [
                (score[at, :, t : t + size] * wide(inv, size)).astype(jnp.bfloat16)
                for t, size in tiles
            ],
            axis=1,
        )
        vals = kv_in[j, :, 1].reshape(seq_len, LANES)
        o = jnp.dot(p, vals, preferred_element_type=jnp.float32)
        cut = [o[i * rows : (i + 1) * rows] for i in range(4)]
        mixed = [jnp.where(low, cut[2 * g], cut[2 * g + 1]) for g in range(2)]
        return jnp.concatenate(crossed(*mixed), axis=1).astype(jnp.bfloat16)

    def a_copy(j, s):
        there = jnp.where(s < 2, z_in, z_out) * 2 + s % 2
        c = y * pairs + j
        return remote(a_out.at[j, s], a_in.at[c], a_send.at[j, s], a_got.at[c], sp=there)

    def relay_first(j):
        beside_came(j)
        kv_across(j, beside).start()
        kv_came(j, 2 + y)
        kv_across(j, 2 + y).start()

    def relay_last(j):
        kv_came(j, 3 - y)
        kv_across(j, 3 - y).start()

        @pl.when(j + 2 < pairs)
        def _():
            kv_across(j + 2, mine).start()

    @pl.when(inner)
    def _():
        relay_first(0)
        relay_last(0)

        def attend(j, carry):
            more = j + 1 < pairs

            @pl.when(more)
            def _():
                relay_first(j + 1)

            for i in range(pairs):
                @pl.when(j == i)
                def _():
                    pass_w(i)
                    if i >= 2:
                        pass_w_aside(i - 2)

            q_came(j, 1 - y)
            q_came(j, 2)
            q_came(j, 3)
            for s in range(4, 8):
                kv_came(j, s)
            order = [2, 3, 1 - y, y]
            multiply_scores(j, order[0], 0)
            for u in range(4):
                if u == 2:
                    @pl.when(more)
                    def _():
                        relay_last(j + 1)

                if u < 3:
                    multiply_scores(j, order[u + 1], (u + 1) % 2)
                exponents(u % 2)
                tile = weigh(j, u % 2)
                if u < 3:
                    a_out[j, order[u]] = tile
                    a_copy(j, order[u]).start()
                else:
                    a_in[y * pairs + j] = tile
            return carry

        lax.fori_loop(0, pairs, attend, 0)
        for i in range(pairs, direct):
            pass_w(i)

    own_w.wait()
    remote(w_ref, w_all.at[core_peer], w_core.at[parts], w_got.at[core_peer, parts], dp=core_peer).wait_recv()

    def a_came(c):
        remote(a_in.at[c], a_in.at[c], a_send.at[0, 0], a_got.at[c], sp=sibling).wait_recv()

    for j in range(pairs):
        a_came((1 - y) * pairs + j)

        @pl.when(outer)
        def _():
            a_came(y * pairs + j)

    for c in range(parts):
        w_came(x_other, c)
    width = w_ref.shape[1]

    def product(shard):
        total = jnp.zeros((rows, width), jnp.float32)
        for c in range(parts):
            total += jnp.dot(
                a_in[c], w_all[shard, c * w_rows : (c + 1) * w_rows, :],
                preferred_element_type=jnp.float32,
            )
        out_ref[:, pl.ds(pl.multiple_of(shard * width, width), width)] = total.astype(jnp.bfloat16)

    for shard in range(m):
        product(shard)

    def sent(j, carry):
        k_aside(j).wait_send()
        v_aside(j).wait_send()
        q_aside(j).wait_send()

        @pl.when(outer)
        def _():
            for s in (mine, beside):
                kv_upward(j, s).wait_send()
                q_upward(j, s).wait_send()

        @pl.when(inner)
        def _():
            for s in range(4):
                kv_across(j, s).wait_send()
            for s in (1 - y, 2, 3):
                a_copy(j, s).wait_send()

        return carry

    lax.fori_loop(0, pairs, sent, 0)
    for i in range(direct):
        w_cross(i).wait_send()
    for i in range(2):
        w_aside(i).wait_send()
    for c in range(parts):
        w_to_core(c).wait_send()
    w_own_core().wait_send()


def rotary_lanes(row_count):
    position = np.arange(row_count)[:, None]
    lane = np.arange(LANES)[None, :]
    place = np.where(lane % HD < HD // 2, position // GRID_W, position % GRID_W).astype(np.float32)
    quarter = HD // 4
    step = (lane % quarter).astype(np.float32)
    inv_freq = np.power(np.float32(rotary_base), -(np.float32(2.0) * step) / np.float32(HD // 2))
    angle = inv_freq.astype(np.float32) * place
    sign = np.where((lane // quarter) % 2 == 0, np.float32(-1.0), np.float32(1.0))
    return np.cos(angle).astype(np.float32), (np.sin(angle) * sign).astype(np.float32)


def on_device(queries, keys, values, q_gain, k_gain, w_out):
    n, m = lax.axis_size("sp"), lax.axis_size("dp")
    rows = queries.shape[2]
    kv_width = keys.shape[1] // 2
    pairs = kv_width // LANES
    if n != 8 or m != 4 or kv_width % LANES or pairs < 2 or rows % 16 or QH != 2 * KV:
        return on_device_plain(queries, keys, values, q_gain, k_gain, w_out)
    seq_len = n * rows
    cos_table, sin_table = rotary_lanes(seq_len)
    hbm = pl.BlockSpec(memory_space=pltpu.HBM)
    bf16, f32 = jnp.bfloat16, jnp.float32
    dma = pltpu.SemaphoreType.DMA
    parts = 2 * pairs
    mixed = pl.pallas_call(
        functools.partial(layer_kernel, m),
        out_shape=jax.ShapeDtypeStruct((rows, w_out.shape[1] * m), bf16),
        in_specs=[hbm] * 8,
        out_specs=pl.BlockSpec(memory_space=pltpu.VMEM),
        scratch_shapes=[
            pltpu.VMEM((rows, queries.shape[1]), bf16),
            pltpu.VMEM((rows, keys.shape[1]), bf16),
            pltpu.VMEM((1, HD), f32),
            pltpu.VMEM((1, HD), f32),
            pltpu.VMEM((rows, LANES), f32),
            pltpu.VMEM((rows, LANES), f32),
            pltpu.VMEM((pairs, rows, LANES), bf16),
            pltpu.VMEM((pairs, rows, 2 * LANES), bf16),
            pltpu.VMEM((pairs, 8, 2, rows, LANES), bf16),
            pltpu.VMEM((pairs, 4, rows, 2 * LANES), bf16),
            pltpu.VMEM((pairs, 4, rows, 2 * LANES), bf16),
            pltpu.VMEM((parts, rows, 2 * LANES), bf16),
            pltpu.VMEM((m, w_out.shape[0], w_out.shape[1]), bf16),
            pltpu.VMEM((2, 4 * rows, seq_len), f32),
            pltpu.VMEM((2, 4 * rows, LANES), f32),
            pltpu.VMEM((2, 4 * rows, LANES), f32),
            dma((6,)), dma((pairs,)), dma((pairs,)), dma((pairs,)), dma((pairs,)),
            dma((pairs,)), dma((pairs,)), dma((pairs, 4)), dma((pairs, 4)), dma((pairs, 4)),
            dma((pairs, 4)), dma((pairs, 8)), dma((pairs, 4)), dma((parts,)),
            dma((parts - 2,)), dma((2,)), dma((parts + 1,)), dma((m, parts + 1)), dma,
        ],
        compiler_params=pltpu.CompilerParams(
            collective_id=0, has_side_effects=True, vmem_limit_bytes=62 * 1024 * 1024
        ),
    )(
        queries[0].T, keys[0].T, values[0].T, q_gain[None], k_gain[None],
        cos_table, sin_table, w_out,
    )
    return mixed[None]


def solution(mesh):
    placed = (
        P("dp", None, "sp"),
        P("dp", None, "sp"),
        P("dp", None, "sp"),
        P(),
        P(),
        P(None, "dp"),
    )
    return jax.shard_map(
        on_device, mesh=mesh, in_specs=placed, out_specs=P("dp", "sp", None), check_vma=False
    )
```

time: 71.1 us -> 54.2 us (0.76)
  the two profiles are of different devices: /device:TPU:9 before, /device:TPU:0 now
where the time goes in v1:
time: 54.2 us; the launch traced here: 53.2 us
  Pallas kernels  51.2 us (94%)
  local copies, waits for them, and re-layouts  1.98 us (4%)
    pallas_call x1, Pallas kernels, on_device(): pl.pallas_call(functools.partial(layer_kernel, m), out_shape=jax.ShapeDty...  51.2 us
    unnamed x1, local copies, waits for them, and re-layouts  1.98 us

profile of v1, /device:TPU:0, one launch (start us, length us, event | category | flops | bytes accessed | tf_op | source)
XLA Modules:
  0.0 53.2 jit_solution(5674740467176668872)
XLA Ops:
  0.0 51.2 %shard_map.82 = bf16[160,2048]{1,0:T(8,128)(2,1)} custom-call(bf16[160,2048]{1,0:T(8,128)(2,1)} %bitcast.13, bf16[160,1024]{1,0:T(8,128)(2,1)} %bitcast.14, bf16[160,1024]{1,0:T(8,128)(2,1)} %bitcast.15, f32[1,64]{1,0:T(1,128)} %bitcast.16, f32[1,64]{1,0:T(1,128)} %bitcast.17, f32[1280,128]{1,0:T(8,128)} %constant.4.clone.cos_ref, ...), custom_call_target="tpu_custom_call" | custom-call | tf_op jit(solution)/shard_map/pallas_call | solution.py:626
  51.2 2.0 %copy.10 = bf16[1,160,2048]{2,1,0:T(8,128)(2,1)} copy(bf16[1,160,2048]{2,1,0:T(8,128)(2,1)} %bitcast.12) | data formatting | bytes 1310720

commit v2 on v1

--- a/solution.py
+++ b/solution.py
@@ -145,7 +145,7 @@
 def layer_kernel(
     m, q_ref, k_ref, v_ref, qg_ref, kg_ref, cos_ref, sin_ref, w_ref, out_ref,
     q_raw, k_raw, q_gain_in, k_gain_in, cos_in, sin_in, k_out, q_out, kv_in, q_in, a_out, a_in,
-    w_all, score, peak, inv_sum,
+    w_all, score, v_turned, summed,
     load, v_own, k_side, v_side, q_side, k_got, v_got, q_got, kv_up, q_up, kv_mid, kv_got,
     a_send, a_got, w_x, w_y, w_core, w_got, w_local,
 ):
@@ -260,12 +260,13 @@
     def w_held(shard, c):
         return w_all.at[shard, pl.ds(pl.multiple_of(c * w_rows, w_rows), w_rows)]
 
-    direct = parts - 2
+    aside = pairs - 1
+    direct = aside + 2
 
     def part_at(i):
-        if i < 2:
+        if i < aside:
             return y * pairs + i
-        return (i % 2) * pairs + 1 + i // 2
+        return (i - aside + 1) * pairs - 1
 
     def w_cross(i):
         c = part_at(i)
@@ -294,7 +295,7 @@
         c = part_at(i)
         w_came(x_peer, c)
         w_to_core(c).start()
-        if i < 2:
+        if i < aside:
             w_aside(i).start()
 
     def pass_w_aside(i):
@@ -415,7 +416,7 @@
         query(pairs - 1)
         for i in range(direct):
             pass_w(i)
-            if i in (2, 3):
+            if i >= 2:
                 pass_w_aside(i - 2)
 
     scale = HD ** (-0.5) * LOG2E
@@ -423,55 +424,46 @@
     seq_len = 8 * rows
     tiles = [(t, min(step, seq_len - t)) for t in range(0, seq_len, step)]
 
-    def halves(tile, op):
-        parts_of = [tile[:, i : i + LANES] for i in range(0, tile.shape[1], LANES)]
-        return functools.reduce(op, parts_of)
-
-    def wide(column, size):
-        return jnp.concatenate([column] * (size // LANES), axis=1)
+    def by_sublane(tile):
+        return tile.reshape(tile.shape[0] // 8, 8, tile.shape[1])
 
     def multiply_scores(j, s, at):
-        stack = []
-        for g in range(2):
-            pair = q_in[j, s, :, g * LANES : (g + 1) * LANES]
-            zero = jnp.zeros_like(pair)
-            stack += [jnp.where(low, pair, zero), jnp.where(low, zero, pair)]
+        pair = [q_in[j, s, :, g * LANES : (g + 1) * LANES] for g in range(2)]
+        zero = jnp.zeros_like(pair[0])
+        stack = [jnp.where(low, one, zero) for one in pair]
+        stack += [jnp.where(low, zero, one) for one in pair]
         stack = jnp.concatenate(stack, axis=0)
         keys = kv_in[j, :, 0].reshape(seq_len, LANES)
         top = None
         for t, size in tiles:
             tile = lax.dot_general(
-                stack, keys[t : t + size], TRANSPOSED, preferred_element_type=jnp.float32
+                keys[t : t + size], stack, TRANSPOSED, preferred_element_type=jnp.float32
             )
-            score[at, :, t : t + size] = tile
-            most = halves(tile, jnp.maximum)
+            score[at, t : t + size] = tile
+            most = jnp.max(by_sublane(tile), axis=0)
             top = most if top is None else jnp.maximum(top, most)
-        peak[at] = jnp.broadcast_to(jnp.max(top, axis=1, keepdims=True), top.shape)
-
-    def exponents(at):
-        top = peak[at]
+        return jnp.max(top, axis=0, keepdims=True)
+
+    def exponents(at, top):
         total = None
         for t, size in tiles:
-            p = jnp.exp2((score[at, :, t : t + size] - wide(top, size)) * scale)
-            score[at, :, t : t + size] = p
-            more = halves(p, jnp.add)
+            p = jnp.exp2((score[at, t : t + size] - top) * scale)
+            score[at, t : t + size] = p
+            more = jnp.sum(by_sublane(p), axis=0)
             total = more if total is None else total + more
-        inv_sum[at] = jnp.broadcast_to(1.0 / jnp.sum(total, axis=1, keepdims=True), total.shape)
-
-    def weigh(j, at):
-        inv = inv_sum[at]
-        p = jnp.concatenate(
-            [
-                (score[at, :, t : t + size] * wide(inv, size)).astype(jnp.bfloat16)
-                for t, size in tiles
-            ],
-            axis=1,
-        )
-        vals = kv_in[j, :, 1].reshape(seq_len, LANES)
-        o = jnp.dot(p, vals, preferred_element_type=jnp.float32)
+        return 1.0 / jnp.sum(total, axis=0, keepdims=True)
+
+    def weigh(at, inv):
+        o = None
+        for t, size in tiles:
+            p = (score[at, t : t + size] * inv).astype(jnp.bfloat16)
+            more = jnp.dot(v_turned[:, t : t + size], p, preferred_element_type=jnp.float32)
+            o = more if o is None else o + more
+        o = o.T
         cut = [o[i * rows : (i + 1) * rows] for i in range(4)]
-        mixed = [jnp.where(low, cut[2 * g], cut[2 * g + 1]) for g in range(2)]
-        return jnp.concatenate(crossed(*mixed), axis=1).astype(jnp.bfloat16)
+        one = jnp.where(low, cut[0], pltpu.roll(cut[1], HD, 1))
+        two = jnp.where(low, pltpu.roll(cut[2], HD, 1), cut[3])
+        return jnp.concatenate([one, two], axis=1).astype(jnp.bfloat16)
 
     def a_copy(j, s):
         there = jnp.where(s < 2, z_in, z_out) * 2 + s % 2
@@ -492,81 +484,105 @@
         def _():
             kv_across(j + 2, mine).start()
 
+    def attend(j):
+        q_came(j, 1 - y)
+        q_came(j, 2)
+        q_came(j, 3)
+        for s in range(4, 8):
+            kv_came(j, s)
+        v_turned[...] = kv_in[j, :, 1].reshape(seq_len, LANES).T
+        order = [2, 3, 1 - y, y]
+        top = multiply_scores(j, order[0], 0)
+        for u in range(4):
+            if u < 3:
+                later = multiply_scores(j, order[u + 1], (u + 1) % 2)
+            inv = exponents(u % 2, top)
+            tile = weigh(u % 2, inv)
+            if u < 3:
+                a_out[j, order[u]] = tile
+                a_copy(j, order[u]).start()
+                top = later
+            else:
+                a_in[y * pairs + j] = tile
+
+    def a_came(c):
+        remote(a_in.at[c], a_in.at[c], a_send.at[0, 0], a_got.at[c], sp=sibling).wait_recv()
+
+    def a_ready(j):
+        a_came((1 - y) * pairs + j)
+
+        @pl.when(outer)
+        def _():
+            a_came(y * pairs + j)
+
+    width = w_ref.shape[1]
+
+    def project(which, first=False, last=False):
+        for shard in range(m):
+            at = slice(shard * width, (shard + 1) * width)
+            total = None if first else summed[:, at]
+            for j in which:
+                for c in (j, pairs + j):
+                    more = jnp.dot(
+                        a_in[c], w_all[shard, c * w_rows : (c + 1) * w_rows, :],
+                        preferred_element_type=jnp.float32,
+                    )
+                    total = more if total is None else total + more
+            if last:
+                out_ref[:, at] = total.astype(jnp.bfloat16)
+            else:
+                summed[:, at] = total
+
+    def w_ready(which):
+        for j in which:
+            for c in (j, pairs + j):
+                w_came(x_other, c)
+
     @pl.when(inner)
     def _():
         relay_first(0)
         relay_last(0)
 
-        def attend(j, carry):
-            more = j + 1 < pairs
-
-            @pl.when(more)
-            def _():
-                relay_first(j + 1)
-
-            for i in range(pairs):
+        def one_pair(j, carry):
+            relay_first(j + 1)
+            relay_last(j + 1)
+            for i in range(pairs - 1):
                 @pl.when(j == i)
                 def _():
                     pass_w(i)
                     if i >= 2:
                         pass_w_aside(i - 2)
 
-            q_came(j, 1 - y)
-            q_came(j, 2)
-            q_came(j, 3)
-            for s in range(4, 8):
-                kv_came(j, s)
-            order = [2, 3, 1 - y, y]
-            multiply_scores(j, order[0], 0)
-            for u in range(4):
-                if u == 2:
-                    @pl.when(more)
-                    def _():
-                        relay_last(j + 1)
-
-                if u < 3:
-                    multiply_scores(j, order[u + 1], (u + 1) % 2)
-                exponents(u % 2)
-                tile = weigh(j, u % 2)
-                if u < 3:
-                    a_out[j, order[u]] = tile
-                    a_copy(j, order[u]).start()
-                else:
-                    a_in[y * pairs + j] = tile
+            attend(j)
             return carry
 
-        lax.fori_loop(0, pairs, attend, 0)
-        for i in range(pairs, direct):
-            pass_w(i)
+        lax.fori_loop(0, pairs - 1, one_pair, 0)
+        for i in range(1, aside - 1):
+            pass_w_aside(i)
 
     own_w.wait()
-    remote(w_ref, w_all.at[core_peer], w_core.at[parts], w_got.at[core_peer, parts], dp=core_peer).wait_recv()
-
-    def a_came(c):
-        remote(a_in.at[c], a_in.at[c], a_send.at[0, 0], a_got.at[c], sp=sibling).wait_recv()
-
-    for j in range(pairs):
-        a_came((1 - y) * pairs + j)
-
-        @pl.when(outer)
-        def _():
-            a_came(y * pairs + j)
-
-    for c in range(parts):
-        w_came(x_other, c)
-    width = w_ref.shape[1]
-
-    def product(shard):
-        total = jnp.zeros((rows, width), jnp.float32)
-        for c in range(parts):
-            total += jnp.dot(
-                a_in[c], w_all[shard, c * w_rows : (c + 1) * w_rows, :],
-                preferred_element_type=jnp.float32,
-            )
-        out_ref[:, pl.ds(pl.multiple_of(shard * width, width), width)] = total.astype(jnp.bfloat16)
-
-    for shard in range(m):
-        product(shard)
+    remote(
+        w_ref, w_all.at[core_peer], w_core.at[parts], w_got.at[core_peer, parts], dp=core_peer
+    ).wait_recv()
+    early = list(range(pairs - 2))
+    w_ready(early)
+    for j in early:
+        a_ready(j)
+    project(early, first=True)
+
+    @pl.when(inner)
+    def _():
+        pass_w(aside)
+        pass_w_aside(aside - 1)
+        attend(pairs - 1)
+        pass_w(aside + 1)
+
+    w_ready([pairs - 2])
+    a_ready(pairs - 2)
+    project([pairs - 2])
+    w_ready([pairs - 1])
+    a_ready(pairs - 1)
+    project([pairs - 1], last=True)
 
     def sent(j, carry):
         k_aside(j).wait_send()
@@ -591,7 +607,7 @@
     lax.fori_loop(0, pairs, sent, 0)
     for i in range(direct):
         w_cross(i).wait_send()
-    for i in range(2):
+    for i in range(aside):
         w_aside(i).wait_send()
     for c in range(parts):
         w_to_core(c).wait_send()
@@ -615,7 +631,7 @@
     rows = queries.shape[2]
     kv_width = keys.shape[1] // 2
     pairs = kv_width // LANES
-    if n != 8 or m != 4 or kv_width % LANES or pairs < 2 or rows % 16 or QH != 2 * KV:
+    if n != 8 or m != 4 or kv_width % LANES or pairs < 3 or rows % 16 or QH != 2 * KV:
         return on_device_plain(queries, keys, values, q_gain, k_gain, w_out)
     seq_len = n * rows
     cos_table, sin_table = rotary_lanes(seq_len)
@@ -642,20 +658,25 @@
             pltpu.VMEM((pairs, 4, rows, 2 * LANES), bf16),
             pltpu.VMEM((parts, rows, 2 * LANES), bf16),
             pltpu.VMEM((m, w_out.shape[0], w_out.shape[1]), bf16),
-            pltpu.VMEM((2, 4 * rows, seq_len), f32),
-            pltpu.VMEM((2, 4 * rows, LANES), f32),
-            pltpu.VMEM((2, 4 * rows, LANES), f32),
+            pltpu.VMEM((2, seq_len, 4 * rows), f32),
+            pltpu.VMEM((LANES, seq_len), bf16),
+            pltpu.VMEM((rows, w_out.shape[1] * m), f32),
             dma((6,)), dma((pairs,)), dma((pairs,)), dma((pairs,)), dma((pairs,)),
             dma((pairs,)), dma((pairs,)), dma((pairs, 4)), dma((pairs, 4)), dma((pairs, 4)),
             dma((pairs, 4)), dma((pairs, 8)), dma((pairs, 4)), dma((parts,)),
-            dma((parts - 2,)), dma((2,)), dma((parts + 1,)), dma((m, parts + 1)), dma,
+            dma((pairs + 1,)), dma((pairs - 1,)), dma((parts + 1,)), dma((m, parts + 1)), dma,
         ],
         compiler_params=pltpu.CompilerParams(
-            collective_id=0, has_side_effects=True, vmem_limit_bytes=62 * 1024 * 1024
+            collective_id=0, has_side_effects=True, vmem_limit_bytes=44 * 1024 * 1024
         ),
     )(
-        queries[0].T, keys[0].T, values[0].T, q_gain[None], k_gain[None],
-        cos_table, sin_table, w_out,
+        *(
+            pltpu.with_memory_space_constraint(x, pltpu.HBM)
+            for x in (
+                queries[0].T, keys[0].T, values[0].T, q_gain[None], k_gain[None],
+                jnp.asarray(cos_table), jnp.asarray(sin_table), w_out,
+            )
+        )
     )
     return mixed[None]
 

time: 54.2 us -> 51.9 us (0.958)
  the two profiles are of different devices: /device:TPU:0 before, /device:TPU:16 now
where the time goes in v2:
time: 51.9 us; the launch traced here: 51.8 us
  Pallas kernels  50.9 us (98%)
  local copies, waits for them, and re-layouts  0.84 us (2%)
    pallas_call x1, Pallas kernels, on_device(): pl.pallas_call(functools.partial(layer_kernel, m), out_shape=jax.ShapeDty...  50.9 us

profile of v2, /device:TPU:16, one launch (start us, length us, event | category | flops | bytes accessed | tf_op | source)
XLA Modules:
  0.0 51.8 jit_solution(14040705256231655377)
XLA Ops:
  0.0 50.9 %shard_map.82 = bf16[160,2048]{1,0:T(8,128)(2,1)S(1)} custom-call(bf16[160,2048]{1,0:T(8,128)(2,1)} %bitcast.13, bf16[160,1024]{1,0:T(8,128)(2,1)} %bitcast.14, bf16[160,1024]{1,0:T(8,128)(2,1)} %bitcast.15, f32[1,64]{1,0:T(1,128)} %bitcast.16, f32[1,64]{1,0:T(1,128)} %bitcast.17, f32[1280,128]{1,0:T(8,128)} %constant.4.clone.cos_ref, ...), custom_call_target="tpu_custom_call" | custom-call | tf_op jit(solution)/shard_map/pallas_call | solution.py:642
  50.9 0.8 %copy.10 = bf16[1,160,2048]{2,1,0:T(8,128)(2,1)} copy(bf16[1,160,2048]{2,1,0:T(8,128)(2,1)S(1)} %bitcast.12) | data formatting | bytes 1310720

commit v3 on v2

--- a/solution.py
+++ b/solution.py
@@ -146,7 +146,7 @@
     m, q_ref, k_ref, v_ref, qg_ref, kg_ref, cos_ref, sin_ref, w_ref, out_ref,
     q_raw, k_raw, q_gain_in, k_gain_in, cos_in, sin_in, k_out, q_out, kv_in, q_in, a_out, a_in,
     w_all, score, v_turned, summed,
-    load, v_own, k_side, v_side, q_side, k_got, v_got, q_got, kv_up, q_up, kv_mid, kv_got,
+    load, v_own, k_side, v_side, q_side, k_got, v_got, q_got, kv_up, q_up, kv_mid, kv_got, kv_low, kv_low_got,
     a_send, a_got, w_x, w_y, w_core, w_got, w_local,
 ):
     me = lax.axis_index("sp")
@@ -169,6 +169,7 @@
     rows = k_raw.shape[0]
     pairs = kv_in.shape[0]
     parts = 2 * pairs
+    shared = pairs // 2
     w_rows = w_ref.shape[0] // parts
 
     barrier = pltpu.get_barrier_semaphore()
@@ -246,6 +247,15 @@
             kv_in.at[j, s], kv_in.at[j, 4 + s], kv_mid.at[j, s], kv_got.at[j, 4 + s], sp=across
         )
 
+    out_same = z_out * 2 + y
+
+    def kv_downward(j, part):
+        at = pl.ds(4 * part, 2 + 2 * part)
+        return remote(
+            kv_in.at[j, at], kv_in.at[j, at], kv_low.at[j, part], kv_low_got.at[j, part],
+            sp=out_same,
+        )
+
     def kv_came(j, s):
         remote(
             kv_in.at[j, s], kv_in.at[j, s], kv_up.at[j, 0], kv_got.at[j, s], sp=across
@@ -376,10 +386,6 @@
         query_step(j)
         q_aside(j).start()
 
-        @pl.when(jnp.logical_and(outer, j == 0))
-        def _():
-            q_upward(j, mine).start()
-
         return carry
 
     w_cross(0).start()
@@ -407,58 +413,73 @@
             q_came(j, beside)
             q_upward(j, beside).start()
 
-        kv(0)
-        query(0)
-        for j in range(1, pairs):
+        for j in range(pairs):
             kv(j)
-            if j > 1:
-                query(j - 1)
-        query(pairs - 1)
-        for i in range(direct):
-            pass_w(i)
-            if i >= 2:
-                pass_w_aside(i - 2)
+        for j in range(shared, pairs):
+            query(j)
 
     scale = HD ** (-0.5) * LOG2E
     step = 2 * LANES
     seq_len = 8 * rows
-    tiles = [(t, min(step, seq_len - t)) for t in range(0, seq_len, step)]
+    near_len = 4 * rows
+
+    def tiles(far):
+        start = near_len * far
+        stop = start + near_len
+        return [(t, min(step, stop - t)) for t in range(start, stop, step)]
 
     def by_sublane(tile):
         return tile.reshape(tile.shape[0] // 8, 8, tile.shape[1])
 
-    def multiply_scores(j, s, at):
+    def exponents(j, s, at, far):
         pair = [q_in[j, s, :, g * LANES : (g + 1) * LANES] for g in range(2)]
         zero = jnp.zeros_like(pair[0])
         stack = [jnp.where(low, one, zero) for one in pair]
         stack += [jnp.where(low, zero, one) for one in pair]
         stack = jnp.concatenate(stack, axis=0)
-        keys = kv_in[j, :, 0].reshape(seq_len, LANES)
+        keys = kv_in[j, 4 * far : 4 * far + 4, 0].reshape(near_len, LANES)
         top = None
-        for t, size in tiles:
+        for t, size in tiles(far):
             tile = lax.dot_general(
-                keys[t : t + size], stack, TRANSPOSED, preferred_element_type=jnp.float32
+                keys[t - near_len * far :][:size], stack, TRANSPOSED, preferred_element_type=jnp.float32
             )
             score[at, t : t + size] = tile
             most = jnp.max(by_sublane(tile), axis=0)
             top = most if top is None else jnp.maximum(top, most)
-        return jnp.max(top, axis=0, keepdims=True)
-
-    def exponents(at, top):
-        total = None
-        for t, size in tiles:
-            p = jnp.exp2((score[at, t : t + size] - top) * scale)
-            score[at, t : t + size] = p
-            more = jnp.sum(by_sublane(p), axis=0)
-            total = more if total is None else total + more
-        return 1.0 / jnp.sum(total, axis=0, keepdims=True)
-
-    def weigh(at, inv):
+        top = jnp.max(top, axis=0, keepdims=True)
+
+        def finish():
+            total = None
+            for t, size in tiles(far):
+                p = jnp.exp2((score[at, t : t + size] - top) * scale)
+                score[at, t : t + size] = p
+                more = jnp.sum(by_sublane(p), axis=0)
+                total = more if total is None else total + more
+            return top, jnp.sum(total, axis=0, keepdims=True)
+
+        return finish
+
+    def staged(j, order, far):
+        found = []
+        ahead = exponents(j, order[0], 0, far)
+        for u in range(len(order)):
+            now = ahead
+            if u + 1 < len(order):
+                ahead = exponents(j, order[u + 1], u + 1, far)
+            found.append(now())
+        return found
+
+    def weigh(at, near, far):
+        top = jnp.maximum(near[0], far[0])
+        shrink = [jnp.exp2((one[0] - top) * scale) for one in (near, far)]
+        inv = 1.0 / (near[1] * shrink[0] + far[1] * shrink[1])
         o = None
-        for t, size in tiles:
-            p = (score[at, t : t + size] * inv).astype(jnp.bfloat16)
-            more = jnp.dot(v_turned[:, t : t + size], p, preferred_element_type=jnp.float32)
-            o = more if o is None else o + more
+        for side in range(2):
+            factor = shrink[side] * inv
+            for t, size in tiles(side):
+                p = (score[at, t : t + size] * factor).astype(jnp.bfloat16)
+                more = jnp.dot(v_turned[:, t : t + size], p, preferred_element_type=jnp.float32)
+                o = more if o is None else o + more
         o = o.T
         cut = [o[i * rows : (i + 1) * rows] for i in range(4)]
         one = jnp.where(low, cut[0], pltpu.roll(cut[1], HD, 1))
@@ -473,6 +494,11 @@
     def relay_first(j):
         beside_came(j)
         kv_across(j, beside).start()
+
+        @pl.when(j < shared)
+        def _():
+            kv_downward(j, 0).start()
+
         kv_came(j, 2 + y)
         kv_across(j, 2 + y).start()
 
@@ -484,26 +510,30 @@
         def _():
             kv_across(j + 2, mine).start()
 
-    def attend(j):
-        q_came(j, 1 - y)
-        q_came(j, 2)
-        q_came(j, 3)
-        for s in range(4, 8):
-            kv_came(j, s)
-        v_turned[...] = kv_in[j, :, 1].reshape(seq_len, LANES).T
-        order = [2, 3, 1 - y, y]
-        top = multiply_scores(j, order[0], 0)
-        for u in range(4):
-            if u < 3:
-                later = multiply_scores(j, order[u + 1], (u + 1) % 2)
-            inv = exponents(u % 2, top)
-            tile = weigh(u % 2, inv)
-            if u < 3:
+    def turn_values(j, far):
+        at = slice(near_len * far, near_len * (far + 1))
+        v_turned[:, at] = kv_in[j, 4 * far : 4 * far + 4, 1].reshape(near_len, LANES).T
+
+    def attend(j, order, await_far, eager):
+        turn_values(j, 0)
+        near = staged(j, order, 0)
+        await_far()
+        turn_values(j, 1)
+        ready = exponents(j, order[0], 0, 1)
+        for u in range(len(order)):
+            far = ready()
+            if u + 1 < len(order):
+                ready = exponents(j, order[u + 1], u + 1, 1)
+            tile = weigh(u, near[u], far)
+            if u + 1 < len(order):
                 a_out[j, order[u]] = tile
-                a_copy(j, order[u]).start()
-                top = later
+                if eager:
+                    a_copy(j, order[u]).start()
             else:
                 a_in[y * pairs + j] = tile
+        if not eager:
+            for s in order[:-1]:
+                a_copy(j, s).start()
 
     def a_came(c):
         remote(a_in.at[c], a_in.at[c], a_send.at[0, 0], a_got.at[c], sp=sibling).wait_recv()
@@ -511,9 +541,10 @@
     def a_ready(j):
         a_came((1 - y) * pairs + j)
 
-        @pl.when(outer)
-        def _():
-            a_came(y * pairs + j)
+        if j >= shared:
+            @pl.when(outer)
+            def _():
+                a_came(y * pairs + j)
 
     width = w_ref.shape[1]
 
@@ -538,28 +569,78 @@
             for c in (j, pairs + j):
                 w_came(x_other, c)
 
+    def far_came(j):
+        for s in range(4, 8):
+            kv_came(j, s)
+
     @pl.when(inner)
     def _():
-        relay_first(0)
-        relay_last(0)
-
-        def one_pair(j, carry):
-            relay_first(j + 1)
-            relay_last(j + 1)
-            for i in range(pairs - 1):
-                @pl.when(j == i)
-                def _():
-                    pass_w(i)
-                    if i >= 2:
-                        pass_w_aside(i - 2)
-
-            attend(j)
-            return carry
-
-        lax.fori_loop(0, pairs - 1, one_pair, 0)
-        for i in range(1, aside - 1):
-            pass_w_aside(i)
-
+        for j in range(shared):
+            relay_first(j)
+            relay_last(j)
+
+    def shared_pair(j, carry):
+        @pl.when(inner)
+        def _():
+            @pl.when(j + shared < pairs)
+            def _():
+                relay_first(j + shared)
+                relay_last(j + shared)
+
+        @pl.when(outer)
+        def _():
+            low_came(j, 0)
+
+        for i in range(shared):
+            @pl.when(j == i)
+            def _():
+                pass_w(i)
+
+        @pl.when(inner)
+        def _():
+            q_came(j, beside)
+
+        def await_far():
+            @pl.when(inner)
+            def _():
+                far_came(j)
+                kv_downward(j, 1).start()
+
+            @pl.when(outer)
+            def _():
+                low_came(j, 1)
+
+        attend(j, [beside, mine], await_far, False)
+        return carry
+
+    def low_came(j, part):
+        kv_downward(j, part).wait_recv()
+
+    @pl.when(outer)
+    def _():
+        for j in range(shared):
+            q_came(j, beside)
+
+    lax.fori_loop(0, shared, shared_pair, 0)
+    order = [2, 3, 1 - y, y]
+
+    def late_pair(j, eager):
+        for s in (1 - y, 2, 3):
+            q_came(j, s)
+        attend(j, order, lambda: far_came(j), eager)
+
+    for i in range(shared, aside):
+        pass_w(i)
+    pass_w_aside(0)
+
+    @pl.when(inner)
+    def _():
+        for j in range(shared, pairs - 1):
+            late_pair(j, False)
+
+    for i in range(1, aside - 1):
+        pass_w_aside(i)
+    pass_w(aside)
     own_w.wait()
     remote(
         w_ref, w_all.at[core_peer], w_core.at[parts], w_got.at[core_peer, parts], dp=core_peer
@@ -569,14 +650,13 @@
     for j in early:
         a_ready(j)
     project(early, first=True)
+    pass_w_aside(aside - 1)
 
     @pl.when(inner)
     def _():
-        pass_w(aside)
-        pass_w_aside(aside - 1)
-        attend(pairs - 1)
-        pass_w(aside + 1)
-
+        late_pair(pairs - 1, True)
+
+    pass_w(aside + 1)
     w_ready([pairs - 2])
     a_ready(pairs - 2)
     project([pairs - 2])
@@ -593,14 +673,29 @@
         def _():
             for s in (mine, beside):
                 kv_upward(j, s).wait_send()
-                q_upward(j, s).wait_send()
+
+                @pl.when(j >= shared)
+                def _():
+                    q_upward(j, s).wait_send()
 
         @pl.when(inner)
         def _():
             for s in range(4):
                 kv_across(j, s).wait_send()
-            for s in (1 - y, 2, 3):
-                a_copy(j, s).wait_send()
+
+            @pl.when(j < shared)
+            def _():
+                for part in range(2):
+                    kv_downward(j, part).wait_send()
+
+            @pl.when(j >= shared)
+            def _():
+                for s in (2, 3):
+                    a_copy(j, s).wait_send()
+
+        @pl.when(jnp.logical_or(inner, j < shared))
+        def _():
+            a_copy(j, beside).wait_send()
 
         return carry
 
@@ -631,7 +726,7 @@
     rows = queries.shape[2]
     kv_width = keys.shape[1] // 2
     pairs = kv_width // LANES
-    if n != 8 or m != 4 or kv_width % LANES or pairs < 3 or rows % 16 or QH != 2 * KV:
+    if n != 8 or m != 4 or kv_width % LANES or pairs < 4 or rows % 32 or QH != 2 * KV:
         return on_device_plain(queries, keys, values, q_gain, k_gain, w_out)
     seq_len = n * rows
     cos_table, sin_table = rotary_lanes(seq_len)
@@ -658,12 +753,13 @@
             pltpu.VMEM((pairs, 4, rows, 2 * LANES), bf16),
             pltpu.VMEM((parts, rows, 2 * LANES), bf16),
             pltpu.VMEM((m, w_out.shape[0], w_out.shape[1]), bf16),
-            pltpu.VMEM((2, seq_len, 4 * rows), f32),
+            pltpu.VMEM((4, seq_len, 4 * rows), f32),
             pltpu.VMEM((LANES, seq_len), bf16),
             pltpu.VMEM((rows, w_out.shape[1] * m), f32),
             dma((6,)), dma((pairs,)), dma((pairs,)), dma((pairs,)), dma((pairs,)),
             dma((pairs,)), dma((pairs,)), dma((pairs, 4)), dma((pairs, 4)), dma((pairs, 4)),
-            dma((pairs, 4)), dma((pairs, 8)), dma((pairs, 4)), dma((parts,)),
+            dma((pairs, 4)), dma((pairs, 8)), dma((pairs, 2)), dma((pairs, 2)), dma((pairs, 4)),
+            dma((parts,)),
             dma((pairs + 1,)), dma((pairs - 1,)), dma((parts + 1,)), dma((m, parts + 1)), dma,
         ],
         compiler_params=pltpu.CompilerParams(

time: 51.9 us -> 54.3 us (1.046)
  the two profiles are of different devices: /device:TPU:16 before, /device:TPU:0 now
where the time goes in v3:
time: 54.3 us; the launch traced here: 53.5 us
  Pallas kernels  52.7 us (97%)
  local copies, waits for them, and re-layouts  0.84 us (2%)
    pallas_call x1, Pallas kernels, on_device(): pl.pallas_call(functools.partial(layer_kernel, m), out_shape=jax.ShapeDty...  52.7 us

profile of v3, /device:TPU:0, one launch (start us, length us, event | category | flops | bytes accessed | tf_op | source)
XLA Modules:
  0.0 53.5 jit_solution(9407865559031524813)
XLA Ops:
  0.0 52.7 %shard_map.82 = bf16[160,2048]{1,0:T(8,128)(2,1)S(1)} custom-call(bf16[160,2048]{1,0:T(8,128)(2,1)} %bitcast.13, bf16[160,1024]{1,0:T(8,128)(2,1)} %bitcast.14, bf16[160,1024]{1,0:T(8,128)(2,1)} %bitcast.15, f32[1,64]{1,0:T(1,128)} %bitcast.16, f32[1,64]{1,0:T(1,128)} %bitcast.17, f32[1280,128]{1,0:T(8,128)} %constant.4.clone.cos_ref, ...), custom_call_target="tpu_custom_call" | custom-call | tf_op jit(solution)/shard_map/pallas_call | solution.py:737
  52.7 0.8 %copy.10 = bf16[1,160,2048]{2,1,0:T(8,128)(2,1)} copy(bf16[1,160,2048]{2,1,0:T(8,128)(2,1)S(1)} %bitcast.12) | data formatting | bytes 1310720

commit v4 on v3

--- a/solution.py
+++ b/solution.py
@@ -270,13 +270,13 @@
     def w_held(shard, c):
         return w_all.at[shard, pl.ds(pl.multiple_of(c * w_rows, w_rows), w_rows)]
 
-    aside = pairs - 1
-    direct = aside + 2
+    aside = pairs // 2
+    direct = parts - aside
 
     def part_at(i):
         if i < aside:
             return y * pairs + i
-        return (i - aside + 1) * pairs - 1
+        return (i % 2) * pairs + (aside + i) // 2
 
     def w_cross(i):
         c = part_at(i)
@@ -592,7 +592,7 @@
             low_came(j, 0)
 
         for i in range(shared):
-            @pl.when(j == i)
+            @pl.when(jnp.logical_and(inner, j == i))
             def _():
                 pass_w(i)
 
@@ -620,6 +620,8 @@
     def _():
         for j in range(shared):
             q_came(j, beside)
+        for i in range(aside + 1):
+            pass_w(i)
 
     lax.fori_loop(0, shared, shared_pair, 0)
     order = [2, 3, 1 - y, y]
@@ -629,8 +631,10 @@
             q_came(j, s)
         attend(j, order, lambda: far_came(j), eager)
 
-    for i in range(shared, aside):
-        pass_w(i)
+    @pl.when(inner)
+    def _():
+        pass_w(aside)
+
     pass_w_aside(0)
 
     @pl.when(inner)
@@ -638,9 +642,10 @@
         for j in range(shared, pairs - 1):
             late_pair(j, False)
 
-    for i in range(1, aside - 1):
+    for i in range(1, aside):
         pass_w_aside(i)
-    pass_w(aside)
+    for i in range(aside + 1, direct - 2):
+        pass_w(i)
     own_w.wait()
     remote(
         w_ref, w_all.at[core_peer], w_core.at[parts], w_got.at[core_peer, parts], dp=core_peer
@@ -650,13 +655,13 @@
     for j in early:
         a_ready(j)
     project(early, first=True)
-    pass_w_aside(aside - 1)
+    pass_w(direct - 2)
 
     @pl.when(inner)
     def _():
         late_pair(pairs - 1, True)
 
-    pass_w(aside + 1)
+    pass_w(direct - 1)
     w_ready([pairs - 2])
     a_ready(pairs - 2)
     project([pairs - 2])
@@ -760,7 +765,7 @@
             dma((pairs,)), dma((pairs,)), dma((pairs, 4)), dma((pairs, 4)), dma((pairs, 4)),
             dma((pairs, 4)), dma((pairs, 8)), dma((pairs, 2)), dma((pairs, 2)), dma((pairs, 4)),
             dma((parts,)),
-            dma((pairs + 1,)), dma((pairs - 1,)), dma((parts + 1,)), dma((m, parts + 1)), dma,
+            dma((parts,)), dma((pairs,)), dma((parts + 1,)), dma((m, parts + 1)), dma,
         ],
         compiler_params=pltpu.CompilerParams(
             collective_id=0, has_side_effects=True, vmem_limit_bytes=44 * 1024 * 1024

time: 54.3 us -> 48.9 us (0.901)
  Pallas kernels: 52.7 us -> 47.1 us
    pallas_call x1, Pallas kernels: 52.7 us -> 47.1 us  [on_device(): pl.pallas_call(functools.partial(layer_kernel, m), out_shape=jax.ShapeDty...]
where the time goes in v4:
time: 48.9 us; the launch traced here: 48 us
  Pallas kernels  47.1 us (96%)
  local copies, waits for them, and re-layouts  0.84 us (2%)
    pallas_call x1, Pallas kernels, on_device(): pl.pallas_call(functools.partial(layer_kernel, m), out_shape=jax.ShapeDty...  47.1 us

profile of v4, /device:TPU:0, one launch (start us, length us, event | category | flops | bytes accessed | tf_op | source)
XLA Modules:
  0.0 48.0 jit_solution(374635541222162390)
XLA Ops:
  0.0 47.1 %shard_map.82 = bf16[160,2048]{1,0:T(8,128)(2,1)S(1)} custom-call(bf16[160,2048]{1,0:T(8,128)(2,1)} %bitcast.13, bf16[160,1024]{1,0:T(8,128)(2,1)} %bitcast.14, bf16[160,1024]{1,0:T(8,128)(2,1)} %bitcast.15, f32[1,64]{1,0:T(1,128)} %bitcast.16, f32[1,64]{1,0:T(1,128)} %bitcast.17, f32[1280,128]{1,0:T(8,128)} %constant.4.clone.cos_ref, ...), custom_call_target="tpu_custom_call" | custom-call | tf_op jit(solution)/shard_map/pallas_call | solution.py:742
  47.2 0.8 %copy.10 = bf16[1,160,2048]{2,1,0:T(8,128)(2,1)} copy(bf16[1,160,2048]{2,1,0:T(8,128)(2,1)S(1)} %bitcast.12) | data formatting | bytes 1310720

commit v5 on v4

--- a/solution.py
+++ b/solution.py
@@ -363,9 +363,8 @@
 
     key_step(0)
     pl.semaphore_wait(barrier, jnp.where(inner, 6, 5))
-    loads[5].wait()
-
-    def send_step(j, carry):
+
+    def key_send(j, carry):
         v_aside(j).start()
 
         @pl.when(j > 0)
@@ -375,7 +374,7 @@
         k_aside(j).start()
         own_values(j).wait()
 
-        @pl.when(jnp.logical_and(outer, j == 0))
+        @pl.when(jnp.logical_and(outer, j < 2))
         def _():
             kv_upward(j, mine).start()
 
@@ -383,14 +382,18 @@
         def _():
             kv_across(j, mine).start()
 
+        return carry
+
+    def query_send(j, carry):
         query_step(j)
         q_aside(j).start()
-
         return carry
 
     w_cross(0).start()
     w_cross(1).start()
-    lax.fori_loop(0, pairs, send_step, 0)
+    lax.fori_loop(0, pairs, key_send, 0)
+    loads[5].wait()
+    lax.fori_loop(0, pairs, query_send, 0)
     for i in range(2, direct):
         w_cross(i).start()
     w_own_core().start()
@@ -402,7 +405,7 @@
     @pl.when(outer)
     def _():
         def kv(j):
-            if j:
+            if j > 1:
                 kv_upward(j, mine).start()
             beside_came(j)
             kv_upward(j, beside).start()
@@ -492,6 +495,10 @@
         return remote(a_out.at[j, s], a_in.at[c], a_send.at[j, s], a_got.at[c], sp=there)
 
     def relay_first(j):
+        @pl.when(j == pairs - 1)
+        def _():
+            kv_across(j, mine).start()
+
         beside_came(j)
         kv_across(j, beside).start()
 
@@ -506,7 +513,7 @@
         kv_came(j, 3 - y)
         kv_across(j, 3 - y).start()
 
-        @pl.when(j + 2 < pairs)
+        @pl.when(j + 3 < pairs)
         def _():
             kv_across(j + 2, mine).start()
 
@@ -626,40 +633,47 @@
     lax.fori_loop(0, shared, shared_pair, 0)
     order = [2, 3, 1 - y, y]
 
-    def late_pair(j, eager):
+    def late_pair(j, eager, await_far=None):
         for s in (1 - y, 2, 3):
             q_came(j, s)
-        attend(j, order, lambda: far_came(j), eager)
+        attend(j, order, await_far or (lambda: far_came(j)), eager)
+
+    early = list(range(pairs - 2))
+
+    def middle_passes():
+        for i in range(aside):
+            pass_w_aside(i)
+        for i in range(aside + 1, direct - 2):
+            pass_w(i)
+        own_w.wait()
+        remote(
+            w_ref, w_all.at[core_peer], w_core.at[parts], w_got.at[core_peer, parts], dp=core_peer
+        ).wait_recv()
+
+    def early_project():
+        w_ready(early)
+        for j in early:
+            a_ready(j)
+        project(early, first=True)
+        pass_w(direct - 2)
 
     @pl.when(inner)
     def _():
         pass_w(aside)
-
-    pass_w_aside(0)
-
-    @pl.when(inner)
-    def _():
         for j in range(shared, pairs - 1):
             late_pair(j, False)
-
-    for i in range(1, aside):
-        pass_w_aside(i)
-    for i in range(aside + 1, direct - 2):
-        pass_w(i)
-    own_w.wait()
-    remote(
-        w_ref, w_all.at[core_peer], w_core.at[parts], w_got.at[core_peer, parts], dp=core_peer
-    ).wait_recv()
-    early = list(range(pairs - 2))
-    w_ready(early)
-    for j in early:
-        a_ready(j)
-    project(early, first=True)
-    pass_w(direct - 2)
-
-    @pl.when(inner)
+        middle_passes()
+
+        def await_last():
+            early_project()
+            far_came(pairs - 1)
+
+        late_pair(pairs - 1, True, await_last)
+
+    @pl.when(outer)
     def _():
-        late_pair(pairs - 1, True)
+        middle_passes()
+        early_project()
 
     pass_w(direct - 1)
     w_ready([pairs - 2])

time: 48.9 us -> 47.2 us (0.965); the launches traced: 48 us -> 46.8 us
  Pallas kernels: 47.1 us -> 46 us
    pallas_call x1, Pallas kernels: 47.1 us -> 46 us  [on_device(): pl.pallas_call(functools.partial(layer_kernel, m), out_shape=jax.ShapeDty...]
where the time goes in v5:
time: 47.2 us; the launch traced here: 46.8 us
  Pallas kernels  46 us (97%)
  local copies, waits for them, and re-layouts  0.84 us (2%)
    pallas_call x1, Pallas kernels, on_device(): pl.pallas_call(functools.partial(layer_kernel, m), out_shape=jax.ShapeDty...  46 us

profile of v5, /device:TPU:0, one launch (start us, length us, event | category | flops | bytes accessed | tf_op | source)
XLA Modules:
  0.0 46.8 jit_solution(4237165926218335818)
XLA Ops:
  0.0 46.0 %shard_map.82 = bf16[160,2048]{1,0:T(8,128)(2,1)S(1)} custom-call(bf16[160,2048]{1,0:T(8,128)(2,1)} %bitcast.13, bf16[160,1024]{1,0:T(8,128)(2,1)} %bitcast.14, bf16[160,1024]{1,0:T(8,128)(2,1)} %bitcast.15, f32[1,64]{1,0:T(1,128)} %bitcast.16, f32[1,64]{1,0:T(1,128)} %bitcast.17, f32[1280,128]{1,0:T(8,128)} %constant.4.clone.cos_ref, ...), custom_call_target="tpu_custom_call" | custom-call | tf_op jit(solution)/shard_map/pallas_call | solution.py:756
  46.0 0.8 %copy.10 = bf16[1,160,2048]{2,1,0:T(8,128)(2,1)} copy(bf16[1,160,2048]{2,1,0:T(8,128)(2,1)S(1)} %bitcast.12) | data formatting | bytes 1310720

commit v6 on v5

--- a/solution.py
+++ b/solution.py
@@ -146,7 +146,7 @@
     m, q_ref, k_ref, v_ref, qg_ref, kg_ref, cos_ref, sin_ref, w_ref, out_ref,
     q_raw, k_raw, q_gain_in, k_gain_in, cos_in, sin_in, k_out, q_out, kv_in, q_in, a_out, a_in,
     w_all, score, v_turned, summed,
-    load, v_own, k_side, v_side, q_side, k_got, v_got, q_got, kv_up, q_up, kv_mid, kv_got, kv_low, kv_low_got,
+    load, v_own, k_side, v_side, q_side, k_got, v_got, q_got, kv_up, q_up, kv_mid, kv_got, kv_low, kv_low_got, v_mid, v_far,
     a_send, a_got, w_x, w_y, w_core, w_got, w_local,
 ):
     me = lax.axis_index("sp")
@@ -495,10 +495,6 @@
         return remote(a_out.at[j, s], a_in.at[c], a_send.at[j, s], a_got.at[c], sp=there)
 
     def relay_first(j):
-        @pl.when(j == pairs - 1)
-        def _():
-            kv_across(j, mine).start()
-
         beside_came(j)
         kv_across(j, beside).start()
 
@@ -576,6 +572,33 @@
             for c in (j, pairs + j):
                 w_came(x_other, c)
 
+    final = pairs - 1
+
+    def k_across(s):
+        return remote(
+            kv_in.at[final, s, 0], kv_in.at[final, 4 + s, 0], kv_mid.at[final, s],
+            kv_got.at[final, 4 + s], sp=across,
+        )
+
+    def v_across(s):
+        return remote(
+            kv_in.at[final, s, 1], kv_in.at[final, 4 + s, 1], v_mid.at[s], v_far.at[s], sp=across
+        )
+
+    def relay(j):
+        if j < final:
+            relay_first(j)
+            relay_last(j)
+            return
+        k_across(mine).start()
+        beside_came(j)
+        k_across(beside).start()
+        for s in (2 + y, 3 - y):
+            kv_came(j, s)
+            k_across(s).start()
+        for s in (mine, beside, 2 + y, 3 - y):
+            v_across(s).start()
+
     def far_came(j):
         for s in range(4, 8):
             kv_came(j, s)
@@ -587,12 +610,10 @@
             relay_last(j)
 
     def shared_pair(j, carry):
-        @pl.when(inner)
-        def _():
-            @pl.when(j + shared < pairs)
+        for i in range(pairs - shared):
+            @pl.when(jnp.logical_and(inner, j == i))
             def _():
-                relay_first(j + shared)
-                relay_last(j + shared)
+                relay(i + shared)
 
         @pl.when(outer)
         def _():
@@ -664,11 +685,24 @@
             late_pair(j, False)
         middle_passes()
 
-        def await_last():
-            early_project()
-            far_came(pairs - 1)
-
-        late_pair(pairs - 1, True, await_last)
+        for s in (1 - y, 2, 3):
+            q_came(final, s)
+        turn_values(final, 0)
+        near = staged(final, order, 0)
+        early_project()
+        for s in range(4):
+            k_across(s).wait_recv()
+        far = staged(final, order, 1)
+        for s in range(4):
+            v_across(s).wait_recv()
+        turn_values(final, 1)
+        for u in range(4):
+            tile = weigh(u, near[u], far[u])
+            if u < 3:
+                a_out[final, order[u]] = tile
+                a_copy(final, order[u]).start()
+            else:
+                a_in[y * pairs + final] = tile
 
     @pl.when(outer)
     def _():
@@ -699,8 +733,10 @@
 
         @pl.when(inner)
         def _():
-            for s in range(4):
-                kv_across(j, s).wait_send()
+            @pl.when(j < pairs - 1)
+            def _():
+                for s in range(4):
+                    kv_across(j, s).wait_send()
 
             @pl.when(j < shared)
             def _():
@@ -719,6 +755,13 @@
         return carry
 
     lax.fori_loop(0, pairs, sent, 0)
+
+    @pl.when(inner)
+    def _():
+        for s in range(4):
+            k_across(s).wait_send()
+            v_across(s).wait_send()
+
     for i in range(direct):
         w_cross(i).wait_send()
     for i in range(aside):
@@ -745,7 +788,7 @@
     rows = queries.shape[2]
     kv_width = keys.shape[1] // 2
     pairs = kv_width // LANES
-    if n != 8 or m != 4 or kv_width % LANES or pairs < 4 or rows % 32 or QH != 2 * KV:
+    if n != 8 or m != 4 or kv_width % LANES or pairs != 4 or rows % 32 or QH != 2 * KV:
         return on_device_plain(queries, keys, values, q_gain, k_gain, w_out)
     seq_len = n * rows
     cos_table, sin_table = rotary_lanes(seq_len)
@@ -777,7 +820,7 @@
             pltpu.VMEM((rows, w_out.shape[1] * m), f32),
             dma((6,)), dma((pairs,)), dma((pairs,)), dma((pairs,)), dma((pairs,)),
             dma((pairs,)), dma((pairs,)), dma((pairs, 4)), dma((pairs, 4)), dma((pairs, 4)),
-            dma((pairs, 4)), dma((pairs, 8)), dma((pairs, 2)), dma((pairs, 2)), dma((pairs, 4)),
+            dma((pairs, 4)), dma((pairs, 8)), dma((pairs, 2)), dma((pairs, 2)), dma((4,)), dma((4,)), dma((pairs, 4)),
             dma((parts,)),
             dma((parts,)), dma((pairs,)), dma((parts + 1,)), dma((m, parts + 1)), dma,
         ],

time: 47.2 us -> 48.3 us (1.023)
  Pallas kernels: 46 us -> 47.4 us
    pallas_call x1, Pallas kernels: 46 us -> 47.4 us  [on_device(): pl.pallas_call(functools.partial(layer_kernel, m), out_shape=jax.ShapeDty...]
where the time goes in v6:
time: 48.3 us; the launch traced here: 48.2 us
  Pallas kernels  47.4 us (98%)
  local copies, waits for them, and re-layouts  0.84 us (2%)
    pallas_call x1, Pallas kernels, on_device(): pl.pallas_call(functools.partial(layer_kernel, m), out_shape=jax.ShapeDty...  47.4 us

profile of v6, /device:TPU:0, one launch (start us, length us, event | category | flops | bytes accessed | tf_op | source)
XLA Modules:
  0.0 48.2 jit_solution(12182180904211886882)
XLA Ops:
  0.0 47.4 %shard_map.82 = bf16[160,2048]{1,0:T(8,128)(2,1)S(1)} custom-call(bf16[160,2048]{1,0:T(8,128)(2,1)} %bitcast.13, bf16[160,1024]{1,0:T(8,128)(2,1)} %bitcast.14, bf16[160,1024]{1,0:T(8,128)(2,1)} %bitcast.15, f32[1,64]{1,0:T(1,128)} %bitcast.16, f32[1,64]{1,0:T(1,128)} %bitcast.17, f32[1280,128]{1,0:T(8,128)} %constant.4.clone.cos_ref, ...), custom_call_target="tpu_custom_call" | custom-call | tf_op jit(solution)/shard_map/pallas_call | solution.py:799
  47.4 0.8 %copy.10 = bf16[1,160,2048]{2,1,0:T(8,128)(2,1)} copy(bf16[1,160,2048]{2,1,0:T(8,128)(2,1)S(1)} %bitcast.12) | data formatting | bytes 1310720

commit v7 on v5

--- a/solution.py
+++ b/solution.py
@@ -211,7 +211,6 @@
     for j in range(pairs):
         own_values(j).start()
     own_w = pltpu.make_async_copy(w_ref, w_all.at[dp], w_local)
-    own_w.start()
 
     def remote(src, dst, sent, got, **there):
         return pltpu.make_async_remote_copy(
@@ -396,6 +395,7 @@
     lax.fori_loop(0, pairs, query_send, 0)
     for i in range(2, direct):
         w_cross(i).start()
+    own_w.start()
     w_own_core().start()
 
     def beside_came(j):

time: 47.2 us -> 47.2 us (level)
  no operation moved by 1% of the time
where the time goes in v7:
time: 47.2 us; the launch traced here: 46.8 us
  Pallas kernels  46 us (97%)
  local copies, waits for them, and re-layouts  0.84 us (2%)
    pallas_call x1, Pallas kernels, on_device(): pl.pallas_call(functools.partial(layer_kernel, m), out_shape=jax.ShapeDty...  46 us

profile of v7, /device:TPU:0, one launch (start us, length us, event | category | flops | bytes accessed | tf_op | source)
XLA Modules:
  0.0 46.8 jit_solution(9140054939279265646)
XLA Ops:
  0.0 46.0 %shard_map.82 = bf16[160,2048]{1,0:T(8,128)(2,1)S(1)} custom-call(bf16[160,2048]{1,0:T(8,128)(2,1)} %bitcast.13, bf16[160,1024]{1,0:T(8,128)(2,1)} %bitcast.14, bf16[160,1024]{1,0:T(8,128)(2,1)} %bitcast.15, f32[1,64]{1,0:T(1,128)} %bitcast.16, f32[1,64]{1,0:T(1,128)} %bitcast.17, f32[1280,128]{1,0:T(8,128)} %constant.4.clone.cos_ref, ...), custom_call_target="tpu_custom_call" | custom-call | tf_op jit(solution)/shard_map/pallas_call | solution.py:756
  46.0 0.8 %copy.10 = bf16[1,160,2048]{2,1,0:T(8,128)(2,1)} copy(bf16[1,160,2048]{2,1,0:T(8,128)(2,1)S(1)} %bitcast.12) | data formatting | bytes 1310720
